TPU v7x, 128 devices: a whole 4x4x4 slice. The times are simulated.
128 devices in a mesh: sp: 16 (over z, y), dp: 8 (over x, core).
Axes of the slice: x: 4, y: 4, z: 4, core: 2. Of those that a mesh axis runs over, the one named last changes fastest.
Arguments:
- inputs: bfloat16 [8, 3072, 2048], P('dp', 'sp'), may hold values from -6 to 6
- in_gain: float32 [2048], replicated, may hold values from 0.1 to 1.9
- w_query: bfloat16 [2048, 1024], P('dp', 'sp'), may hold values from -0.125 to 0.125
- w_key: bfloat16 [2048, 256], P('dp', 'sp'), may hold values from -0.375 to 0.375
- w_value: bfloat16 [2048, 256], P('dp', 'sp'), may hold values from -0.125 to 0.125
- key_bias: float32 [8, 3072, 16], P('dp', None, 'sp'), may hold values from -20 to 0
- out_gain: float32 [1024], replicated, may hold values from 0.1 to 1.9
- w_out: bfloat16 [1024, 2048], P('sp', 'dp'), may hold values from -0.1875 to 0.1875
Outputs:
- mixed: bfloat16 [8, 3072, 2048], P('dp', 'sp')
All inputs are finite; a program needn't handle non-finite values.
Results may differ from a plain program's by a relative error of at most 0.012.
The roundings to bfloat16 on the way count: a program that leaves them out, or rounds other values in their place, can miss the bound.
Values may be sent and summed in bfloat16 or wider, within the bound.
A program may use at most 128 MiB of HBM per device.

v0:
```python
import jax
import jax.numpy as jnp
from jax import lax
from jax.sharding import PartitionSpec as P

HEAD_DIM = 64


norm_eps = 1e-06


def rows_first(arrays, axis, dims):
    turned = [jnp.moveaxis(a, dim, 0) for a, dim in zip(arrays, dims)]
    both = jnp.concatenate([t.reshape(len(t), -1) for t in turned], axis=1)
    whole, at, finished = (lax.all_gather(both, axis, axis=0, tiled=True), 0, [])
    for t, dim in zip(turned, dims):
        slab = whole[:, at : at + t[0].size].reshape(-1, *t.shape[1:])
        finished.append(jnp.moveaxis(slab, 0, dim))
        at += t[0].size
    return tuple(finished)


def sent_together(arrays, axis, split_dim, concat_dim, along):
    ends, at = ([], 0)
    for a in arrays[:-1]:
        at += a.shape[along]
        ends.append(at)
    both = jnp.concatenate(arrays, axis=along)
    return tuple(
        jnp.split(
            lax.all_to_all(both, axis, split_axis=split_dim, concat_axis=concat_dim, tiled=True),
            ends,
            axis=along,
        )
    )


def body(inputs, in_gain, w_query, w_key, w_value, key_bias, out_gain, w_out):
    width_sp = lax.axis_size("sp")
    own_index = lax.axis_index("sp")
    wide = inputs[0].astype(jnp.float32)
    normed_rows = (
        wide * lax.rsqrt(jnp.mean(wide * wide, axis=-1, keepdims=True) + norm_eps) * in_gain
    ).astype(jnp.bfloat16)
    local_rows = normed_rows.shape[0]
    w_query, w_key, w_value, w_out = rows_first(
        (w_query, w_key, w_value, w_out), "dp", (0, 0, 0, 1)
    )
    w_key, w_value = rows_first((w_key, w_value), "sp", (1, 1))
    keys = jnp.dot(normed_rows, w_key, preferred_element_type=jnp.float32).astype(jnp.bfloat16)
    values = jnp.dot(normed_rows, w_value, preferred_element_type=jnp.float32).astype(jnp.bfloat16)
    queries = jnp.dot(
        normed_rows,
        lax.all_gather(w_query, "sp", axis=1, tiled=True),
        preferred_element_type=jnp.float32,
    ).astype(jnp.bfloat16)
    heads_here = key_bias.shape[2]
    kv_heads = keys.shape[1] // HEAD_DIM
    spread = width_sp // kv_heads
    query_slots = queries.reshape(local_rows, width_sp, heads_here * HEAD_DIM)
    key_copies = jnp.repeat(keys.reshape(local_rows, kv_heads, HEAD_DIM), spread, axis=1)
    value_copies = jnp.repeat(values.reshape(local_rows, kv_heads, HEAD_DIM), spread, axis=1)
    query_all, key_all, value_all = sent_together(
        (query_slots, key_copies, value_copies), "sp", 1, 0, 2
    )
    keys_head = key_all[:, 0, :]
    values_head = value_all[:, 0, :]
    length_all = query_all.shape[0]
    bias_here = key_bias[0].T
    block = min(512, length_all)
    pieces = []
    for index in range(length_all // block):
        start = index * block
        end = start + block
        logits = jnp.einsum(
            "thd,sd->hts", query_all[start:end], keys_head[:end], preferred_element_type=jnp.float32
        )
        logits = logits * HEAD_DIM ** (-0.5) + bias_here[:, None, :end]
        rows = start + jnp.arange(block, dtype=jnp.int32)[:, None]
        columns = jnp.arange(end, dtype=jnp.int32)[None, :]
        strict = (columns < rows)[None, :, :]
        log_keep = jnp.where(strict, jax.nn.log_sigmoid(-logits), jnp.float32(0.0))
        log_rest = lax.cumsum(log_keep, axis=2, reverse=True) - log_keep
        sticks = jnp.where(
            strict, jnp.exp(jax.nn.log_sigmoid(logits) + log_rest), jnp.float32(0.0)
        ).astype(jnp.bfloat16)
        pieces.append(
            jnp.einsum("hts,sd->thd", sticks, values_head[:end], preferred_element_type=jnp.float32)
        )
    attended = jnp.concatenate(pieces, axis=0)
    gains = lax.dynamic_slice_in_dim(
        out_gain, own_index * heads_here * HEAD_DIM, heads_here * HEAD_DIM, 0
    )
    scaled = attended * lax.rsqrt(jnp.mean(attended * attended, axis=-1, keepdims=True) + norm_eps)
    head_out = (scaled * gains.reshape(heads_here, HEAD_DIM)).astype(jnp.bfloat16)
    returned = lax.all_to_all(head_out, "sp", split_axis=0, concat_axis=1, tiled=True)
    returned = returned.reshape(local_rows, width_sp * heads_here * HEAD_DIM)
    mixed = jnp.dot(
        returned,
        lax.all_gather(w_out, "sp", axis=0, tiled=True),
        preferred_element_type=jnp.float32,
    )
    return mixed.astype(jnp.bfloat16)[None]


def solution(mesh):
    placed = (
        P("dp", "sp", None),
        P(),
        P("dp", "sp"),
        P("dp", "sp"),
        P("dp", "sp"),
        P("dp", None, "sp"),
        P(),
        P("sp", "dp"),
    )
    return jax.shard_map(
        body, mesh=mesh, in_specs=placed, out_specs=P("dp", "sp", None), check_vma=False
    )
```

profile of v0, /device:TPU:96, one launch (start us, length us, event | category | flops | bytes accessed | tf_op | source)
XLA Modules:
  0.0 346.5 jit_solution(17781443614021492482)
XLA Ops:
  7.4 13.6 %all_gather.12 = bf16[2048,160]{0,1:T(8,128)(2,1)S(1)} all-gather(bf16[256,160]{0,1:T(8,128)(2,1)S(1)} %pad_maximum_fusion.2), channel_id=1, replica_groups=mesh['sp'=16,'dp'=8] {'dp'}, dimensions={0}, use_global_device_ids=true | all-gather | bytes 737280 | tf_op jit(solution)/shard_map/all_gather | solution.py:15
  22.9 44.2 %all-gather.6.cloned.1.call-done = bf16[256,4096]{1,0:T(8,128)(2,1)} async-done(((bf16[16,4096]{1,0:T(8,128)(2,1)}), bf16[256,4096]{1,0:T(8,128)(2,1)}) %all-gather.6.cloned.1.call-update) | async-done | bytes 2097168 | tf_op jit(solution)/shard_map/all_gather | solution.py:15
  69.7 50.6 %all-gather.4.cloned.1.call-done = bf16[2048,1024]{0,1:T(8,128)(2,1)} async-done(((bf16[2048,64]{0,1:T(8,128)(2,1)}), bf16[2048,1024]{0,1:T(8,128)(2,1)}) %all-gather.4.cloned.1.call-update) | async-done | bytes 4194320 | tf_op jit(solution)/shard_map/all_gather | solution.py:54
  125.8 5.7 %all-to-all-start = ((bf16[192,16,192]{0,2,1:T(8,128)(2,1)}), bf16[192,16,192]{0,2,1:T(8,128)(2,1)S(1)}, u32[]{:S(2)}, u32[]{:S(2)}) async-start(bf16[192,16,192]{0,2,1:T(8,128)(2,1)} %pad_maximum_fusion), calls=%async_computation | async-start | bytes 3145728 | tf_op jit(solution)/shard_map/all_to_all | solution.py:31
  133.2 21.8 %all-to-all-done = bf16[192,16,192]{0,2,1:T(8,128)(2,1)S(1)} async-done(((bf16[192,16,192]{0,2,1:T(8,128)(2,1)}), bf16[192,16,192]{0,2,1:T(8,128)(2,1)S(1)}, u32[]{:S(2)}, u32[]{:S(2)}) %all-to-all-start) | async-done | bytes 1179680 | tf_op jit(solution)/shard_map/all_to_all | solution.py:31
  159.1 4.8 %fusion.121 = f32[1,512,4,128]{1,2,3,0:T(4,128)S(1)} fusion(f32[1,512,4,128]{1,3,2,0:T(8,128)S(1)} %bitcast.409), kind=kOutput, calls=%fused_computation.155 | output fusion | flops 33292288 | bytes 2097152 | tf_op jit(solution)/shard_map/reduce-window
  168.1 5.2 %fusion.74 = f32[1,512,8,128]{1,2,3,0:T(8,128)S(1)} fusion(f32[1,512,8,128]{1,3,2,0:T(8,128)S(1)} %bitcast.404), kind=kOutput, calls=%fused_computation.113 | output fusion | flops 66584576 | bytes 4194304 | tf_op jit(solution)/shard_map/reduce-window.2
  180.0 10.1 %fusion.42 = f32[1,512,12,128]{1,2,3,0:T(8,128)S(1)} fusion(f32[1,512,12,128]{1,3,2,0:T(8,128)S(1)} %bitcast.402), kind=kOutput, calls=%fused_computation.69 | output fusion | flops 99876864 | bytes 6291456 | tf_op jit(solution)/shard_map/reduce-window.4
  192.0 6.1 %fusion.34 = (f32[1,512,2048]{1,2,0:T(8,128)S(1)}, f32[2048,512]{1,0:T(8,128)}) fusion(f32[2048]{0:T(1024)S(1)} %bitcast.419, s32[512]{0:T(512)S(1)} %iota_add_fusion.2, bf16[3072,1,192]{0,2,1:T(8,128)(2,1)} %copy-done.1), kind=kOutput, calls=%fused_computation.56 | convolution fusion | flops 145752064 | bytes 8726528 | tf_op jit(solution)/shard_map/thd,sd->hts/dot_general | solution.py:75
  198.1 10.5 %fusion.40 = f32[1,512,16,128]{1,2,3,0:T(8,128)S(1)} fusion(f32[1,512,16,128]{1,3,2,0:T(8,128)S(1)} %bitcast.401), kind=kOutput, calls=%fused_computation.67 | output fusion | flops 133169152 | bytes 8388608 | tf_op jit(solution)/shard_map/reduce-window.6
  208.6 4.4 %copy.67 = f32[1,512,16,128]{1,3,2,0:T(8,128)} copy(f32[1,512,16,128]{1,2,3,0:T(8,128)S(1)} %fusion.40) | data formatting | bytes 8388608 | tf_op jit(solution)/shard_map/reduce-window.6
  213.1 7.1 %fusion.22 = (f32[1,512,2560]{1,2,0:T(8,128)S(1)}, f32[2560,512,1]{1,0,2:T(8,128)}) fusion(s32[512]{0:T(512)S(1)} %iota_add_fusion.1, f32[2560]{0:T(1024)S(1)} %slice_reduce_fusion, bf16[3072,1,192]{0,2,1:T(8,128)(2,1)} %copy-done.1), kind=kOutput, calls=%fused_computation.38 | convolution fusion | flops 182190080 | bytes 10891264 | tf_op jit(solution)/shard_map/thd,sd->hts/dot_general | solution.py:75
  220.2 15.3 %fusion.14 = f32[1,512,20,128]{1,2,3,0:T(8,128)S(1)} fusion(f32[1,512,20,128]{1,3,2,0:T(8,128)S(1)} %bitcast.400), kind=kOutput, calls=%fused_computation.27 | output fusion | flops 166461440 | bytes 10485760 | tf_op jit(solution)/shard_map/reduce-window.8
  235.5 5.4 %copy.69 = f32[1,512,20,128]{1,3,2,0:T(8,128)} copy(f32[1,512,20,128]{1,2,3,0:T(8,128)S(1)} %fusion.14) | data formatting | bytes 10485760 | tf_op jit(solution)/shard_map/reduce-window.8
  241.0 8.2 %fusion.6 = (f32[1,512,3072]{1,2,0:T(8,128)S(1)}, f32[3072,512]{1,0:T(8,128)}) fusion(f32[3072]{0:T(1024)S(1)} %bitcast.417, s32[512]{0:T(512)S(1)} %iota_add_fusion, bf16[3072,1,192]{0,2,1:T(8,128)(2,1)} %copy-done.1), kind=kOutput, calls=%fused_computation.14 | convolution fusion | flops 218628096 | bytes 13056000 | tf_op jit(solution)/shard_map/thd,sd->hts/dot_general | solution.py:75
  249.2 15.5 %fusion.12 = f32[1,512,24,128]{1,2,3,0:T(8,128)S(1)} fusion(f32[1,512,24,128]{1,3,2,0:T(8,128)S(1)} %bitcast.398), kind=kOutput, calls=%fused_computation.25 | output fusion | flops 199753728 | bytes 12582912 | tf_op jit(solution)/shard_map/reduce-window.10
  264.7 6.3 %copy.71 = f32[1,512,24,128]{1,3,2,0:T(8,128)} copy(f32[1,512,24,128]{1,2,3,0:T(8,128)S(1)} %fusion.12) | data formatting | bytes 12582912 | tf_op jit(solution)/shard_map/reduce-window.10
  273.9 5.8 %fusion.64 = bf16[1,512,1024]{1,2,0:T(8,128)(2,1)S(1)} fusion(f32[1,512,8,128]{1,3,2,0:T(8,128)} %copy.63, f32[1024,512]{1,0:T(8,128)} %get-tuple-element.12, f32[512,8]{0,1:T(8,128)S(1)} %slice_bitcast_fusion.47, f32[1024]{0:T(1024)S(1)} %bitcast.423, s32[512]{0:T(512)S(1)} %iota_add_fusion.4), kind=kLoop, calls=%fused_computation.98 | loop fusion | flops 12582912 | bytes 5265408 | tf_op jit(solution)/shard_map/convert_element_type | solution.py:86
  279.7 6.4 %fusion.51 = bf16[1,512,1536]{1,2,0:T(8,128)(2,1)S(1)} fusion(f32[1,512,12,128]{1,3,2,0:T(8,128)S(1)} %copy.65, f32[1,512,1536]{1,2,0:T(8,128)} %get-tuple-element.14, f32[512,12]{0,1:T(8,128)S(1)} %slice_bitcast_fusion.45, s32[512]{0:T(512)S(1)} %iota_add_fusion.3), kind=kLoop, calls=%fused_computation.80 | loop fusion | flops 17301504 | bytes 7890944 | tf_op jit(solution)/shard_map/convert_element_type | solution.py:86
  286.1 7.3 %fusion.32 = bf16[1,512,2048]{1,2,0:T(8,128)(2,1)S(1)} fusion(f32[1,512,16,128]{1,3,2,0:T(8,128)S(1)} %copy-done, f32[2048,512]{1,0:T(8,128)S(1)} %copy-done.3, f32[512,16]{0,1:T(8,128)S(1)} %slice_bitcast_fusion.43, f32[2048]{0:T(1024)S(1)} %bitcast.420, s32[512]{0:T(512)S(1)} %iota_add_fusion.2), kind=kLoop, calls=%fused_computation.54 | loop fusion | flops 25165824 | bytes 10528768 | tf_op jit(solution)/shard_map/convert_element_type | solution.py:86
  293.4 9.8 %fusion.20 = bf16[1,512,2560]{1,2,0:T(8,128)(2,1)S(1)} fusion(f32[1,512,20,128]{1,3,2,0:T(8,128)S(1)} %bitcast.395, f32[2560,512,1]{1,0,2:T(8,128)} %get-tuple-element.18, f32[512,20]{0,1:T(8,128)S(1)} %slice_bitcast_fusion.41, s32[512]{0:T(512)S(1)} %iota_add_fusion.1), kind=kLoop, calls=%fused_computation.36 | loop fusion | flops 28835840 | bytes 13150208 | tf_op jit(solution)/shard_map/convert_element_type | solution.py:86
  303.4 10.8 %fusion.4 = bf16[1,512,3072]{1,2,0:T(8,128)(2,1)S(1)} fusion(f32[1,512,24,128]{1,3,2,0:T(8,128)S(1)} %bitcast.393, f32[3072,512]{1,0:T(8,128)S(1)} %bitcast.397, f32[512,24]{0,1:T(8,128)S(1)} %slice_bitcast_fusion.39, f32[3072]{0:T(1024)S(1)} %bitcast.418, s32[512]{0:T(512)S(1)} %iota_add_fusion), kind=kLoop, calls=%fused_computation.12 | loop fusion | flops 37748736 | bytes 15792128 | tf_op jit(solution)/shard_map/convert_element_type | solution.py:86
  319.5 13.0 %all_to_all.33 = bf16[16,2,6144]{2,1,0:T(2,128)(2,1)S(1)} all-to-all(bf16[16,2,6144]{2,1,0:T(2,128)(2,1)S(1)} %reshape.777), channel_id=1, replica_groups=mesh['sp'=16,'dp'=8] {'sp'}, dimensions={0} | all-to-all | bytes 786432 | tf_op jit(solution)/shard_map/all_to_all | solution.py:96
  335.6 4.1 %fusion.59 = bf16[1,192,2048]{2,1,0:T(8,128)(2,1)} fusion(bf16[192,1024]{0,1:T(8,128)(2,1)S(1)} %bitcast.408, bf16[1024,2048]{1,0:T(8,128)(2,1)} %all-gather.8.cloned.1.call-done), kind=kOutput, calls=%fused_computation.93 | convolution fusion | flops 805699584 | bytes 5373952 | tf_op jit(solution)/shard_map/dot_general | solution.py:98
  (108 shorter events, 40.7 us)
Async XLA Ops:
  6.5 16.1 %copy-start.4 = (bf16[1,192,2048]{2,1,0:T(8,128)(2,1)S(1)}, bf16[1,192,2048]{2,1,0:T(8,128)(2,1)}, u32[]{:S(2)}) copy-start(bf16[1,192,2048]{2,1,0:T(8,128)(2,1)} %param.8) | copy-start | bytes 2359300
  6.5 60.5 %copy-start.7 = (f32[2048]{0:T(1024)S(1)}, f32[2048]{0:T(1024)}, u32[]{:S(2)}) copy-start(f32[2048]{0:T(1024)} %param.9) | copy-start | bytes 24580
  6.5 60.5 %all-gather.6.cloned.1.call-start = ((), (), s32[]{:S(2)}) async-start(), calls=%async_computation.3 | async-start | bytes 2228224 | tf_op jit(solution)/shard_map/all_gather | solution.py:15
  21.7 98.6 %all-gather.4.cloned.1.call-start = ((), (), s32[]{:S(2)}) async-start(), calls=%async_computation.2 | async-start | bytes 4456448 | tf_op jit(solution)/shard_map/all_gather | solution.py:54
  67.0 2.0 copy-start.6
  124.3 7.9 %copy-start.5 = (f32[1,3072,1]{1,2,0:T(1,128)S(1)}, f32[1,3072,1]{1,2,0:T(1,128)}, u32[]{:S(2)}) copy-start(f32[1,3072,1]{1,2,0:T(1,128)} %param.13) | copy-start | bytes 36868
  125.8 29.1 %all-to-all-start = ((bf16[192,16,192]{0,2,1:T(8,128)(2,1)}), bf16[192,16,192]{0,2,1:T(8,128)(2,1)S(1)}, u32[]{:S(2)}, u32[]{:S(2)}) async-start(bf16[192,16,192]{0,2,1:T(8,128)(2,1)} %pad_maximum_fusion), calls=%async_computation | async-start | bytes 3145728 | tf_op jit(solution)/shard_map/all_to_all | solution.py:31
  131.5 204.1 %all-gather.8.cloned.1.call-start = ((), (), s32[]{:S(2)}) async-start(), calls=%async_computation.4 | async-start | bytes 4456448 | tf_op jit(solution)/shard_map/all_gather | solution.py:100
  157.5 18.4 %copy-start.1 = (bf16[3072,1,192]{0,2,1:T(8,128)(2,1)}, bf16[3072,1,192]{0,2,1:T(8,128)(2,1)S(1)}, u32[]{:S(2)}) copy-start(bf16[3072,1,192]{0,2,1:T(8,128)(2,1)S(1)} %all_to_all.27) | copy-start | bytes 3538948
  271.2 14.8 %copy-start.3 = (f32[2048,512]{1,0:T(8,128)S(1)}, f32[2048,512]{1,0:T(8,128)}, u32[]{:S(2)}) copy-start(f32[2048,512]{1,0:T(8,128)} %get-tuple-element.16) | copy-start | bytes 12582916
  273.9 19.5 %slice-start.2 = ((s8[5242880]{0:T(1024)(128)(4,1)}), s8[4194304]{0:T(1024)(128)(4,1)S(1)}, s32[]{:S(2)}) async-start(s8[5242880]{0:T(1024)(128)(4,1)} %bitcast.394), calls=%async_computation.7 | async-start | bytes 8388608
  279.7 6.4 %copy-start = (f32[1,512,16,128]{1,3,2,0:T(8,128)S(1)}, f32[1,512,16,128]{1,3,2,0:T(8,128)}, u32[]{:S(2)}) copy-start(f32[1,512,16,128]{1,3,2,0:T(8,128)} %copy.67) | copy-start | bytes 12582916
  279.7 13.7 %slice-start.3 = ((s8[5242880]{0:T(1024)(128)(4,1)}), s8[1048576]{0:T(1024)(128)(4,1)S(1)}, s32[]{:S(2)}) async-start(s8[5242880]{0:T(1024)(128)(4,1)} %bitcast.394), calls=%async_computation.8 | async-start | bytes 2097152
  286.1 17.2 %slice-start = ((s8[6291456]{0:T(1024)(128)(4,1)}), s8[4194304]{0:T(1024)(128)(4,1)S(1)}, s32[]{:S(2)}) async-start(s8[6291456]{0:T(1024)(128)(4,1)} %bitcast.392), calls=%async_computation.5 | async-start | bytes 8388608
  286.1 17.2 %slice-start.4 = ((s8[6291456]{0:T(1024)(128)(4,1)}), s8[2097152]{0:T(1024)(128)(4,1)S(1)}, s32[]{:S(2)}) async-start(s8[6291456]{0:T(1024)(128)(4,1)} %bitcast.396), calls=%async_computation.9 | async-start | bytes 4194304
  293.4 9.9 %slice-start.1 = ((s8[6291456]{0:T(1024)(128)(4,1)}), s8[2097152]{0:T(1024)(128)(4,1)S(1)}, s32[]{:S(2)}) async-start(s8[6291456]{0:T(1024)(128)(4,1)} %bitcast.392), calls=%async_computation.6 | async-start | bytes 4194304
  293.4 9.9 %slice-start.5 = ((s8[6291456]{0:T(1024)(128)(4,1)}), s8[4194304]{0:T(1024)(128)(4,1)S(1)}, s32[]{:S(2)}) async-start(s8[6291456]{0:T(1024)(128)(4,1)} %bitcast.396), calls=%async_computation.10 | async-start | bytes 8388608
  303.4 10.9 %copy-start.2 = (bf16[3072,1,192]{0,2,1:T(8,128)(2,1)S(1)}, bf16[3072,1,192]{0,2,1:T(8,128)(2,1)}, u32[]{:S(2)}) copy-start(bf16[3072,1,192]{0,2,1:T(8,128)(2,1)} %copy-done.1) | copy-start | bytes 3538948
Sparse Core Ops, SparseCore 0:
  21.8 45.1 all-gather.5
  69.2 51.0 all-gather.3
  134.5 54.5 all-gather.7
where the time goes:
time: 353 us; the launch traced here: 346 us
  waiting for transfers between devices  117 us (33%)
  other arithmetic  109 us (31%)
  matrix products  42.7 us (12%)
  local copies, waits for them, and re-layouts  31.2 us (9%)
  blocking collectives  26.6 us (8%)
  between operations  13.9 us (4%)
  starting transfers between devices  5.96 us (2%)
    another operation x12, other arithmetic  61.9 us
    all_gather x1, waiting for transfers between devices, body(): lax.all_gather(w_query, 'sp', axis=1, tiled=True)  50.6 us
    all_gather x1, waiting for transfers between devices, rows_first(): lax.all_gather(both, axis, axis=0, tiled=True)  44.2 us
    convert_element_type x6, other arithmetic, body(): sticks = jnp.where(strict, jnp.exp(jax.nn.log_sigmoid(logits) + log_rest)...  42.7 us
    dot_general x6, matrix products, body(): jnp.einsum('thd,sd->hts', query_all[start:end], keys_head[:end], preferre...  29.9 us
    another operation x18, local copies, waits for them, and re-layouts  21.8 us
    all_to_all x1, waiting for transfers between devices, sent_together(): lax.all_to_all(both, axis, split_axis=split_dim, concat_axis=concat_dim,...  21.8 us
    all_gather x1, blocking collectives, rows_first(): lax.all_gather(both, axis, axis=0, tiled=True)  13.6 us
  transfers between devices with their start and end apart: 4, of which 3 were waited for; matrix products, arithmetic and copies ran while one was open for 49% of the time, Pallas kernels for 0%

commit v1 on v0

v1 whole, which is shorter than its diff:
```python
import functools

import jax
import jax.numpy as jnp
from jax import lax
from jax.experimental import pallas as pl
from jax.experimental.pallas import tpu as pltpu
from jax.sharding import PartitionSpec as P

HEAD_DIM = 64
RING = 4
EPS = 1e-06
LOG2E = 1.4426950408889634
F32 = jnp.float32
BF16 = jnp.bfloat16
MESH = pl.DeviceIdType.MESH


def rcopy(src, dst, send, recv, device):
    return pltpu.make_async_remote_copy(
        src_ref=src, dst_ref=dst, send_sem=send, recv_sem=recv, device_id=device, device_id_type=MESH
    )


def places():
    sp, dp = lax.axis_index("sp"), lax.axis_index("dp")
    z, y = lax.div(sp, RING), lax.rem(sp, RING)
    x, c = lax.div(dp, 2), lax.rem(dp, 2)

    def at(dz=0, dy=0, dx=0, dc=0):
        nz, ny = lax.rem(z + dz, RING), lax.rem(y + dy, RING)
        nx, nc = lax.rem(x + dx, RING), lax.rem(c + dc, 2)
        return {"sp": nz * RING + ny, "dp": nx * 2 + nc}

    return z, y, x, c, at


def project_kernel(
    x_ref, gain_ref, wq_ref, wk_ref, wv_ref,
    qv_ref, kk_ref,
    packs, w_all, xg, stage_qv, stage_k,
    wy_s, wy_r, wx_s, wx_r, wf_s, wf_r, wc_s, wc_r, xd_s, xd_r, xf_s, xf_r, a_s, a_r, b_s, b_r,
):
    z, y, x, c, at = places()
    rows = x_ref.shape[0]
    half = rows // 2
    depth = wq_ref.shape[0]
    packs[c, x, y] = jnp.concatenate(
        [wq_ref[...], wk_ref[...], wv_ref[...], jnp.zeros((depth, 32), BF16)], axis=1
    )
    friends = [at(dz=1), at(dz=3), at(dy=1), at(dy=2), at(dy=3), at(dx=1), at(dx=3), at(dc=1)]
    barrier = pltpu.get_barrier_semaphore()
    for f in friends:
        pl.semaphore_signal(barrier, inc=1, device_id=f, device_id_type=MESH)
    pl.semaphore_wait(barrier, len(friends))

    sent = []

    def go(copy):
        copy.start()
        sent.append(copy)

    lo, hi = pl.ds(0, half), pl.ds(half, half)
    x_right = [rcopy(x_ref.at[p], xg.at[0, p], xd_s.at[0, i], xd_r.at[0, i], at(dz=1)) for i, p in enumerate((lo, hi))]
    x_left = [rcopy(x_ref.at[p], xg.at[1, p], xd_s.at[1, i], xd_r.at[1, i], at(dz=3)) for i, p in enumerate((hi, lo))]
    go(x_right[0])
    go(x_left[0])

    def piece(o):
        return lax.rem(y + RING - o, RING)

    wy = [None] + [
        rcopy(packs.at[c, x, y], packs.at[c, x, y], wy_s.at[o], wy_r.at[o], at(dy=o)) for o in (1, 2, 3)
    ]

    def from_y(o):
        p = packs.at[c, x, piece(o)]
        return rcopy(p, p, wy_s.at[o], wy_r.at[o], at(dy=o))

    def along_x(o, d):
        p = packs.at[c, x, piece(o)]
        return rcopy(p, p, wx_s.at[d, o], wx_r.at[d, o], at(dx=1 if d == 0 else 3))

    def arrived_x(o, d):
        nx = lax.rem(x + (3 if d == 0 else 1), RING)
        p = packs.at[c, nx, piece(o)]
        return rcopy(p, p, wx_s.at[d, o], wx_r.at[d, o], at(dx=1 if d == 0 else 3))

    def far_x(o, d, source_dx):
        nx = lax.rem(x + source_dx, RING)
        part = packs.at[c, nx, piece(o), pl.ds(0 if d == 0 else depth // 2, depth // 2)]
        return rcopy(part, part, wf_s.at[d, o], wf_r.at[d, o], at(dx=1 if d == 0 else 3))

    def across(dx):
        nx = lax.rem(x + dx, RING)
        slab = packs.at[c, nx]
        return rcopy(slab, slab, wc_s.at[dx], wc_r.at[dx], at(dc=1))

    def across_in(dx):
        nx = lax.rem(x + dx, RING)
        slab = packs.at[1 - c, nx]
        return rcopy(slab, slab, wc_s.at[dx], wc_r.at[dx], at(dc=1))

    for o in (1, 3, 2):
        go(wy[o])
    for d in (0, 1):
        go(along_x(0, d))
    go(x_right[1])
    go(x_left[1])
    for o in (1, 3, 2):
        from_y(o).wait_recv()
        for d in (0, 1):
            go(along_x(o, d))
    go(across(0))
    for o in (0, 1, 3, 2):
        for d in (0, 1):
            arrived_x(o, d).wait_recv()
            go(far_x(o, d, 3 if d == 0 else 1))
    go(across(3))
    go(across(1))
    cuts = ((0, 64), (64, 32))
    xg_in = lambda d, i: rcopy(
        xg.at[d, (lo, hi)[i if d == 0 else 1 - i]], xg.at[d, (lo, hi)[i if d == 0 else 1 - i]],
        xd_s.at[d, i], xd_r.at[d, i], at(dz=1 if d == 0 else 3),
    )

    def far_z(d, i):
        a, n = cuts[i]
        part = pl.ds(a + (0 if d == 0 else half), n)
        return rcopy(xg.at[d, part], xg.at[2, part], xf_s.at[d, i], xf_r.at[d, i], at(dz=1 if d == 0 else 3))

    def far_in(d, i):
        a, n = cuts[i]
        part = pl.ds(a + (0 if d == 0 else half), n)
        return rcopy(xg.at[2, part], xg.at[2, part], xf_s.at[d, i], xf_r.at[d, i], at(dz=1 if d == 0 else 3))

    for d in (0, 1):
        xg_in(d, 0).wait_recv()
        for i in (0, 1):
            go(far_z(d, i))
    for o in (0, 1, 3, 2):
        for d in (0, 1):
            far_x(o, d, 2).wait_recv()
    go(across(2))
    for dx in (0, 3, 1, 2):
        across_in(dx).wait_recv()

    for n in range(2 * RING):
        p = [packs[n % 2, n // 2, i] for i in range(RING)]
        at_rows = pl.ds(n * depth, depth)
        w_all[at_rows, 0:128] = jnp.concatenate([p[0][:, 0:64], p[1][:, 0:64]], axis=1)
        w_all[at_rows, 128:256] = jnp.concatenate([p[2][:, 0:64], p[3][:, 0:64]], axis=1)
        w_all[at_rows, 256:384] = jnp.concatenate(
            [t[:, 64:80] for t in p] + [t[:, 80:96] for t in p], axis=1
        )

    def chunk(n, source, first, count, stage_at, dz):
        wide = source.astype(F32)
        normed = (
            wide * lax.rsqrt(jnp.mean(wide * wide, axis=-1, keepdims=True) + EPS) * gain_ref[...]
        ).astype(BF16)
        out = jnp.dot(normed, w_all[...], preferred_element_type=F32).astype(BF16)
        v = out[:, 320:384]
        k = out[:, 256:320].reshape(count // 32, 2, 16, HEAD_DIM)
        here = pl.ds(stage_at, count)
        here_k = pl.ds(stage_at // 2, count // 2)
        for i in range(RING):
            stage_qv[i, here] = jnp.concatenate([out[:, i * 64 : i * 64 + 64], v], axis=1)
        stage_k[here_k] = jnp.concatenate([k[:, 0], k[:, 1]], axis=2).reshape(count // 2, 128)
        nz = lax.rem(z + dz, RING)

        def spot(dy, halved):
            ny = lax.rem(y + dy, RING)
            start = (nz * RING + ny) * rows + first
            if halved:
                return pl.ds(pl.multiple_of(lax.div(start, 2), 16), count // 2)
            return pl.ds(pl.multiple_of(start, 32), count)

        for o in (1, 3, 2):
            ny = lax.rem(y + o, RING)
            go(rcopy(stage_qv.at[ny, here], qv_ref.at[spot(0, False)], a_s.at[n, o], a_r.at[n, o], at(dy=o)))
            go(rcopy(stage_k.at[here_k], kk_ref.at[spot(0, True)], b_s.at[n, o], b_r.at[n, o], at(dy=o)))
        qv_ref[spot(0, False)] = stage_qv[y, here]
        kk_ref[spot(0, True)] = stage_k[here_k]
        waits = []
        for o in (1, 3, 2):
            s, t = qv_ref.at[spot(RING - o, False)], kk_ref.at[spot(RING - o, True)]
            waits.append(rcopy(s, s, a_s.at[n, o], a_r.at[n, o], at(dy=o)))
            waits.append(rcopy(t, t, b_s.at[n, o], b_r.at[n, o], at(dy=o)))
        return waits

    pending = chunk(0, x_ref[...], 0, rows, 0, 0)
    pending += chunk(1, xg[0, lo], 0, half, rows, 3)
    pending += chunk(2, xg[1, hi], half, half, rows + half, 1)
    xg_in(0, 1).wait_recv()
    pending += chunk(3, xg[0, hi], half, half, 2 * rows, 3)
    xg_in(1, 1).wait_recv()
    pending += chunk(4, xg[1, lo], 0, half, 2 * rows + half, 1)
    n, place = 5, 3 * rows
    for i in (0, 1):
        a, count = cuts[i]
        for d in (0, 1):
            far_in(d, i).wait_recv()
            first = a + (0 if d == 0 else half)
            pending += chunk(n, xg[2, pl.ds(first, count)], first, count, place, 2)
            n, place = n + 1, place + count
    for w in pending:
        w.wait_recv()
    for s in sent:
        s.wait_send()


def project(x, gain, wq, wk, wv):
    rows, width = x.shape
    length = rows * RING * RING
    depth = wq.shape[0]
    dma = pltpu.SemaphoreType.DMA
    vmem = pl.BlockSpec(memory_space=pltpu.VMEM)
    return pl.pallas_call(
        project_kernel,
        name="project",
        out_shape=(
            jax.ShapeDtypeStruct((length, 128), BF16),
            jax.ShapeDtypeStruct((length // 2, 128), BF16),
        ),
        in_specs=[vmem] * 5,
        out_specs=(vmem, vmem),
        scratch_shapes=[
            pltpu.VMEM((2, RING, RING, depth, 128), BF16),
            pltpu.VMEM((width, 384), BF16),
            pltpu.VMEM((3, rows, width), BF16),
            pltpu.VMEM((RING, RING * rows, 128), BF16),
            pltpu.VMEM((RING * rows // 2, 128), BF16),
            dma((4,)), dma((4,)), dma((2, 4)), dma((2, 4)), dma((2, 4)), dma((2, 4)), dma((4,)), dma((4,)),
            dma((2, 2)), dma((2, 2)), dma((2, 2)), dma((2, 2)),
            dma((9, 4)), dma((9, 4)), dma((9, 4)), dma((9, 4)),
        ],
        compiler_params=pltpu.CompilerParams(
            collective_id=0, has_side_effects=True, vmem_limit_bytes=48 << 20
        ),
    )(x, gain, wq, wk, wv)


BLOCK_Q = 768
BLOCK_K = 256


def attend_kernel(qv_ref, kk_ref, b_ref, g_ref, o_ref, keys_t, qa, vv, tri, acc, car):
    length = qv_ref.shape[0]
    r = lax.broadcasted_iota(jnp.int32, (BLOCK_K, BLOCK_K), 0)
    c = lax.broadcasted_iota(jnp.int32, (BLOCK_K, BLOCK_K), 1)
    tri[...] = jnp.where(r > c, 1.0, 0.0).astype(BF16)
    step = 512

    @pl.loop(0, length // step)
    def _(i):
        rows = pl.ds(pl.multiple_of(i * step, step), step)
        packed = kk_ref[pl.ds(pl.multiple_of(i * (step // 2), step // 2), step // 2), :]
        packed = packed.reshape(step // 32, 16, 128)
        k = jnp.concatenate([packed[:, :, 0:64], packed[:, :, 64:128]], axis=1).reshape(step, HEAD_DIM)
        kk = k.astype(F32) * (LOG2E / 8.0)
        hi = kk.astype(BF16)
        lo = (kk - hi.astype(F32)).astype(BF16)
        keys_t[0:128, rows] = jnp.concatenate([hi, lo], axis=1).T
        bb = b_ref[0:1, rows] * LOG2E
        bh = bb.astype(BF16)
        r1 = bb - bh.astype(F32)
        bm = r1.astype(BF16)
        bl = (r1 - bm.astype(F32)).astype(BF16)
        keys_t[128:144, rows] = jnp.concatenate([bh, bm, bl, jnp.zeros((13, step), BF16)], axis=0)
        both = qv_ref[rows, :]
        qq = both[:, 0:64]
        lane = lax.broadcasted_iota(jnp.int32, (step, 128), 1)
        qa[rows, 0:128] = jnp.concatenate([qq, qq], axis=1)
        qa[rows, 128:256] = jnp.where(lane < 3, 1.0, 0.0).astype(BF16)
        vv[rows, :] = both[:, 64:128]

    ratio = BLOCK_Q // BLOCK_K

    @pl.loop(0, length // BLOCK_Q)
    def _(i):
        rows = pl.ds(pl.multiple_of(i * BLOCK_Q, BLOCK_Q), BLOCK_Q)
        q = qa[rows, 0:144]

        def one(j, carry, diagonal=None):
            cols = pl.ds(pl.multiple_of(j * BLOCK_K, BLOCK_K), BLOCK_K)
            l2 = jnp.dot(q, keys_t[:, cols], preferred_element_type=F32)
            if diagonal is not None:
                t = lax.broadcasted_iota(jnp.int32, (BLOCK_Q, BLOCK_K), 0)
                s = lax.broadcasted_iota(jnp.int32, (BLOCK_Q, BLOCK_K), 1)
                l2 = jnp.where(s + diagonal < t, l2, -1e30)
            mx = jnp.maximum(l2, 0.0)
            mn = jnp.minimum(l2, 0.0)
            log_part = jnp.log2(1.0 + jnp.exp2(mn - mx))
            drop = (mx + log_part).astype(BF16)
            after = jnp.dot(drop, tri[...], preferred_element_type=F32)
            x = (mn - log_part) - after - jnp.concatenate([carry] * (BLOCK_K // 128), axis=1)
            sticks = jnp.exp2(x).astype(BF16)
            pv = jnp.dot(sticks, vv[cols, :], preferred_element_type=F32)
            whole = after[:, 0:1] + drop[:, 0:128].astype(F32)[:, 0:1]
            return pv, carry + jnp.broadcast_to(whole, carry.shape)

        carry = jnp.zeros((BLOCK_Q, 128), F32)
        total = jnp.zeros((BLOCK_Q, HEAD_DIM), F32)
        for d in reversed(range(ratio)):
            pv, carry = one(i * ratio + d, carry, d * BLOCK_K)
            total = total + pv
        acc[...] = total
        car[...] = carry
        full = i * ratio
        odd = lax.rem(full, 2)

        def single(n, _):
            pv, after = one(full - 1 - n, car[...])
            acc[...] += pv
            car[...] = after
            return 0

        lax.fori_loop(0, odd, single, 0)

        def double(n, _):
            base = full - 1 - odd - n * 2
            pv0, cc = one(base, car[...])
            pv1, cc = one(base - 1, cc)
            acc[...] += pv0 + pv1
            car[...] = cc
            return 0

        lax.fori_loop(0, lax.div(full, 2), double, 0)
        a = acc[...]
        scaled = a * lax.rsqrt(jnp.mean(a * a, axis=-1, keepdims=True) + EPS)
        o_ref[rows, :] = (scaled * g_ref[...]).astype(BF16)


def attend(qv, kk, bias, gain):
    length = qv.shape[0]
    vmem = pl.BlockSpec(memory_space=pltpu.VMEM)
    return pl.pallas_call(
        attend_kernel,
        name="attend",
        out_shape=jax.ShapeDtypeStruct((length, HEAD_DIM), BF16),
        in_specs=[vmem] * 4,
        out_specs=vmem,
        scratch_shapes=[
            pltpu.VMEM((144, length), BF16),
            pltpu.VMEM((length, 256), BF16),
            pltpu.VMEM((length, HEAD_DIM), BF16),
            pltpu.VMEM((BLOCK_K, BLOCK_K), BF16),
            pltpu.VMEM((BLOCK_Q, HEAD_DIM), F32),
            pltpu.VMEM((BLOCK_Q, 128), F32),
        ],
        compiler_params=pltpu.CompilerParams(vmem_limit_bytes=48 << 20),
    )(qv, kk, bias, gain)


def body(inputs, in_gain, w_query, w_key, w_value, key_bias, out_gain, w_out):
    rows = inputs.shape[1]
    width_sp = lax.axis_size("sp")
    own = lax.axis_index("sp")
    qv, kk = project(inputs[0], in_gain[None], w_query, w_key, w_value)
    gain = lax.dynamic_slice_in_dim(out_gain, own * HEAD_DIM, HEAD_DIM, 0)[None]
    head_out = attend(qv, kk, key_bias[0].T, gain)
    returned = lax.all_to_all(head_out, "sp", split_axis=0, concat_axis=1, tiled=True)
    w_out = lax.all_gather(w_out, "dp", axis=1, tiled=True)
    w_out = lax.all_gather(w_out, "sp", axis=0, tiled=True)
    mixed = jnp.dot(returned, w_out, preferred_element_type=F32)
    return mixed.astype(BF16)[None]


def solution(mesh):
    placed = (
        P("dp", "sp", None), P(), P("dp", "sp"), P("dp", "sp"), P("dp", "sp"),
        P("dp", None, "sp"), P(), P("sp", "dp"),
    )
    return jax.shard_map(body, mesh=mesh, in_specs=placed, out_specs=P("dp", "sp", None), check_vma=False)
```

time: 353 us -> 120 us (0.34)
  the two profiles are of different devices: /device:TPU:96 before, /device:TPU:0 now
where the time goes in v1:
time: 120 us; the launch traced here: 119 us
  Pallas kernels  68.5 us (57%)
  blocking collectives  27.8 us (23%)
  between operations  13.4 us (11%)
  local copies, waits for them, and re-layouts  5.48 us (5%)
  matrix products  4.09 us (3%)
    pallas_call x1, Pallas kernels, project(): pl.pallas_call(project_kernel, name='project', out_shape=(jax.ShapeDtypeS...  49.7 us
    pallas_call x1, Pallas kernels, attend(): pl.pallas_call(attend_kernel, name='attend', out_shape=jax.ShapeDtypeStru...  18.9 us
    all_gather x1, blocking collectives, body(): w_out = lax.all_gather(w_out, 'dp', axis=1, tiled=True)  14.7 us
    all_to_all x1, blocking collectives, body(): lax.all_to_all(head_out, 'sp', split_axis=0, concat_axis=1, tiled=True)  13.1 us
    unnamed x11, local copies, waits for them, and re-layouts  5.05 us
    dot_general x1, matrix products, body(): mixed = jnp.dot(returned, w_out, preferred_element_type=F32)  4.09 us
  transfers between devices with their start and end apart: 1, of which 0 were waited for; matrix products, arithmetic and copies ran while one was open for 2% of the time, Pallas kernels for 57%

profile of v1, /device:TPU:0, one launch (start us, length us, event | category | flops | bytes accessed | tf_op | source)
XLA Modules:
  0.0 119.4 jit_solution(8231883446298684194)
XLA Ops:
  6.5 0.0 copy-start
  6.5 0.0 all-gather.2.cloned.1.call-start
  6.5 14.7 %all_gather.6 = bf16[64,2048]{1,0:T(8,128)(2,1)} all-gather(bf16[64,256]{1,0:T(8,128)(2,1)} %param.15), channel_id=1, replica_groups=mesh['sp'=16,'dp'=8] {'dp'}, dimensions={1}, use_global_device_ids=true | all-gather | bytes 294912 | tf_op jit(solution)/shard_map/all_gather | solution.py:364
  21.2 0.0 all-gather.2.cloned.1.call-update
  21.3 0.9 copy.12.wq_ref
  22.2 0.8 copy.13.wk_ref
  23.0 0.8 copy.14.wv_ref
  23.8 0.0 copy-start.1
  23.8 1.1 copy-done.1
  24.9 0.0 copy-start.3
  24.9 0.7 copy-done.3
  25.6 49.7 %project.1 = (bf16[3072,128]{1,0:T(8,128)(2,1)S(1)}, bf16[1536,128]{1,0:T(8,128)(2,1)S(1)}) custom-call(bf16[192,2048]{1,0:T(8,128)(2,1)S(1)} %bitcast.14, f32[1,2048]{1,0:T(1,128)S(1)} %bitcast.16, bf16[256,64]{1,0:T(8,128)(2,1)S(1)} %copy.12.wq_ref, bf16[256,16]{1,0:T(8,128)(2,1)S(1)} %copy.13.wk_ref, bf16[256,16]{1,0:T(8,128)(2,1)S(1)} %copy.14.wv_ref), custom_call_target="tpu_custom_call" | custom-call | tf_op jit(solution)/shard_map/project/pallas_call | solution.py:219
  75.3 0.0 copy-done
  75.3 0.1 dynamic-slice_bitcast_fusion.g_ref
  75.4 0.0 copy-start.2
  75.4 0.7 copy-done.2
  76.1 18.9 %attend.1 = bf16[3072,64]{1,0:T(8,128)(2,1)S(1)} custom-call(bf16[3072,128]{1,0:T(8,128)(2,1)S(1)} %get-tuple-element.7.qv_ref, bf16[1536,128]{1,0:T(8,128)(2,1)S(1)} %get-tuple-element.8.kk_ref, f32[1,3072]{1,0:T(1,128)S(1)} %bitcast.15, f32[1,64]{1,0:T(1,128)S(1)} %dynamic-slice_bitcast_fusion.g_ref), custom_call_target="tpu_custom_call" | custom-call | tf_op jit(solution)/shard_map/attend/pallas_call | solution.py:338
  95.0 0.3 copy.15
  95.3 13.1 %all_to_all.19 = bf16[16,192,64]{1,2,0:T(8,128)(2,1)S(1)} all-to-all(bf16[16,192,64]{1,2,0:T(8,128)(2,1)S(1)} %copy.15), channel_id=1, replica_groups=mesh['sp'=16,'dp'=8] {'sp'}, dimensions={0} | all-to-all | bytes 786432 | tf_op jit(solution)/shard_map/all_to_all | solution.py:363
  108.4 0.0 all-gather.2.cloned.1.call-done
  108.4 4.1 %fusion = bf16[1,192,2048]{2,1,0:T(8,128)(2,1)} fusion(bf16[192,1024]{0,1:T(8,128)(2,1)S(1)} %bitcast.17, bf16[1024,2048]{1,0:T(8,128)(2,1)} %all-gather.2.cloned.1.call-done), kind=kOutput, calls=%fused_computation.1 | convolution fusion | flops 805699584 | bytes 5373952 | tf_op jit(solution)/shard_map/dot_general | solution.py:366
Async XLA Ops:
  6.5 68.8 %copy-start = (f32[1024]{0:T(1024)S(1)}, f32[1024]{0:T(1024)}, u32[]{:S(2)}) copy-start(f32[1024]{0:T(1024)} %param.14) | copy-start | bytes 12292
  6.5 101.9 %all-gather.2.cloned.1.call-start = ((), (), s32[]{:S(2)}) async-start(), calls=%async_computation.1 | async-start | bytes 4456448 | tf_op jit(solution)/shard_map/all_gather | solution.py:365
  23.8 1.1 copy-start.1
  24.9 0.7 copy-start.3
  75.4 0.7 copy-start.2
Sparse Core Ops, SparseCore 0:
  21.4 61.0 all-gather.1

commit v2 on v1

v2 whole, which is shorter than its diff:
```python
import functools

import jax
import jax.numpy as jnp
from jax import lax
from jax.experimental import pallas as pl
from jax.experimental.pallas import tpu as pltpu
from jax.sharding import PartitionSpec as P

HEAD_DIM = 64
RING = 4
EPS = 1e-06
LOG2E = 1.4426950408889634
F32 = jnp.float32
BF16 = jnp.bfloat16
MESH = pl.DeviceIdType.MESH


def rcopy(src, dst, send, recv, device):
    return pltpu.make_async_remote_copy(
        src_ref=src, dst_ref=dst, send_sem=send, recv_sem=recv, device_id=device, device_id_type=MESH
    )


def places():
    sp, dp = lax.axis_index("sp"), lax.axis_index("dp")
    z, y = lax.div(sp, RING), lax.rem(sp, RING)
    x, c = lax.div(dp, 2), lax.rem(dp, 2)

    def at(dz=0, dy=0, dx=0, dc=0):
        nz, ny = lax.rem(z + dz, RING), lax.rem(y + dy, RING)
        nx, nc = lax.rem(x + dx, RING), lax.rem(c + dc, 2)
        return {"sp": nz * RING + ny, "dp": nx * 2 + nc}

    return z, y, x, c, at


def project_kernel(
    x_ref, gain_ref, wq_ref, wk_ref, wv_ref, wo_in,
    qv_ref, kk_ref, wo_ref,
    packs, w_all, xg, stage_qv, stage_k,
    wy_s, wy_r, wx_s, wx_r, wf_s, wf_r, wc_s, wc_r, xd_s, xd_r, xf_s, xf_r, a_s, a_r, b_s, b_r,
    oz_s, oz_r, oy_s, oy_r, ox_s, ox_r, of_s, of_r, oc_s, oc_r, local_sem,
):
    z, y, x, c, at = places()
    rows = x_ref.shape[0]
    half = rows // 2
    depth = wq_ref.shape[1]
    qn, kn = wq_ref.shape[0], wk_ref.shape[0]
    piece_rows = qn + 2 * kn
    packs[c, x, y] = jnp.concatenate([wq_ref[...], wk_ref[...], wv_ref[...]], axis=0)
    friends = [at(dz=1), at(dz=3), at(dy=1), at(dy=2), at(dy=3), at(dx=1), at(dx=3), at(dc=1)]
    barrier = pltpu.get_barrier_semaphore()
    for f in friends:
        pl.semaphore_signal(barrier, inc=1, device_id=f, device_id_type=MESH)

    def wo_cols(dx, cc):
        return pl.ds(pl.multiple_of((lax.rem(x + dx, RING) * 2 + cc) * depth, depth), depth)

    own_wo = pltpu.make_async_copy(wo_in, wo_ref.at[y, z, :, wo_cols(0, c)], local_sem)
    own_wo.start()
    pl.semaphore_wait(barrier, len(friends))

    sent = []

    def go(copy):
        copy.start()
        sent.append(copy)

    def near(d, axis):
        return at(**{axis: 1 if d == 0 else 3})

    def back(d):
        return 3 if d == 0 else 1

    lo, hi = pl.ds(0, half), pl.ds(half, half)
    halves = (lo, hi)

    def oz(dz, n):
        return wo_ref.at[y, lax.rem(z + dz, RING), n, wo_cols(0, c)]

    every, top, low = pl.ds(0, 64), pl.ds(0, 32), pl.ds(32, 32)
    go_oz = [rcopy(wo_in, oz(0, every), oz_s.at[d, 0], oz_r.at[d, 0], near(d, "dz")) for d in (0, 1)]

    def oz_in(d):
        s = oz(back(d), every)
        return rcopy(s, s, oz_s.at[d, 0], oz_r.at[d, 0], near(d, "dz"))

    def oz_far(d, dz):
        s = oz(dz, top if d == 0 else low)
        return rcopy(s, s, oz_s.at[d, 1], oz_r.at[d, 1], near(d, "dz"))

    def x_out(d, i):
        p = halves[i if d == 0 else 1 - i]
        return rcopy(x_ref.at[p], xg.at[d, p], xd_s.at[d, i], xd_r.at[d, i], near(d, "dz"))

    def x_in(d, i):
        p = halves[i if d == 0 else 1 - i]
        return rcopy(xg.at[d, p], xg.at[d, p], xd_s.at[d, i], xd_r.at[d, i], near(d, "dz"))

    cuts = ((0, 64), (64, 32))

    def far_z(d, i, arrived):
        a, n = cuts[i]
        part = pl.ds(a + (0 if d == 0 else half), n)
        return rcopy(xg.at[2 if arrived else d, part], xg.at[2, part], xf_s.at[d, i], xf_r.at[d, i], near(d, "dz"))

    def piece(o):
        return lax.rem(y + RING - o, RING)

    def w_y(o, arrived):
        p = packs.at[c, x, piece(o) if arrived else y]
        return rcopy(p, p, wy_s.at[o], wy_r.at[o], at(dy=o))

    def w_x(o, d, arrived):
        p = packs.at[c, lax.rem(x + back(d), RING) if arrived else x, piece(o)]
        return rcopy(p, p, wx_s.at[d, o], wx_r.at[d, o], near(d, "dx"))

    def w_far(o, d, dx):
        part = packs.at[c, lax.rem(x + dx, RING), piece(o), pl.ds(0 if d == 0 else piece_rows // 2, piece_rows // 2)]
        return rcopy(part, part, wf_s.at[d, o], wf_r.at[d, o], near(d, "dx"))

    def w_c(dx, arrived):
        slab = packs.at[1 - c if arrived else c, lax.rem(x + dx, RING)]
        return rcopy(slab, slab, wc_s.at[dx], wc_r.at[dx], at(dc=1))

    def oy(d, arrived):
        s = wo_ref.at[lax.rem(y + back(d), RING) if arrived else y, :, :, wo_cols(0, c)]
        return rcopy(s, s, oy_s.at[d, 0], oy_r.at[d, 0], near(d, "dy"))

    def oy_far(d, dy):
        s = wo_ref.at[lax.rem(y + dy, RING), pl.ds(0 if d == 0 else 2, 2), :, wo_cols(0, c)]
        return rcopy(s, s, oy_s.at[d, 1], oy_r.at[d, 1], near(d, "dy"))

    def ox(o, d, arrived):
        s = wo_ref.at[piece(o), :, :, wo_cols(back(d) if arrived else 0, c)]
        return rcopy(s, s, ox_s.at[d, o], ox_r.at[d, o], near(d, "dx"))

    def ox_far(o, d, dx):
        s = wo_ref.at[piece(o), pl.ds(0 if d == 0 else 2, 2), :, wo_cols(dx, c)]
        return rcopy(s, s, of_s.at[d, o], of_r.at[d, o], near(d, "dx"))

    def oc(dx, arrived):
        s = wo_ref.at[:, :, :, wo_cols(dx, 1 - c if arrived else c)]
        return rcopy(s, s, oc_s.at[dx], oc_r.at[dx], at(dc=1))

    with jax.named_scope("issue"):
        for o in (1, 3, 2):
            go(w_y(o, False))
        for d in (0, 1):
            go(w_x(0, d, False))
        for d in (0, 1):
            go(go_oz[d])
        for i in (0, 1):
            for d in (0, 1):
                go(x_out(d, i))
    with jax.named_scope("wait_wy"):
        for o in (1, 3, 2):
            w_y(o, True).wait_recv()
            for d in (0, 1):
                go(w_x(o, d, False))
        go(w_c(0, False))
    with jax.named_scope("wait_oz"):
        own_wo.wait()
        for d in (0, 1):
            oz_in(d).wait_recv()
            go(oz_far(d, back(d)))
    with jax.named_scope("wait_wx"):
        for o in (0, 1, 3, 2):
            for d in (0, 1):
                w_x(o, d, True).wait_recv()
                go(w_far(o, d, back(d)))
        go(w_c(3, False))
        go(w_c(1, False))
    with jax.named_scope("wait_ozfar"):
        for d in (0, 1):
            oz_far(d, 2).wait_recv()
        for d in (0, 1):
            go(oy(d, False))
            go(ox(0, d, False))
    with jax.named_scope("wait_wfar"):
        for o in (0, 1, 3, 2):
            for d in (0, 1):
                w_far(o, d, 2).wait_recv()
        go(w_c(2, False))
    with jax.named_scope("wait_x0"):
        for d in (0, 1):
            x_in(d, 0).wait_recv()
            for i in (0, 1):
                go(far_z(d, i, False))
    with jax.named_scope("wait_wc"):
        for dx in (0, 3, 1, 2):
            w_c(dx, True).wait_recv()

    with jax.named_scope("assemble"):
        for n in range(2 * RING):
            cols = pl.ds(n * depth, depth)
            for i in range(RING):
                p = packs[n % 2, n // 2, i]
                w_all[i * qn : (i + 1) * qn, cols] = p[0:qn]
                w_all[RING * qn + i * kn : RING * qn + (i + 1) * kn, cols] = p[qn : qn + kn]
                w_all[RING * (qn + kn) + i * kn : RING * (qn + kn) + (i + 1) * kn, cols] = p[qn + kn :]

    def chunk(n, source, first, count, stage_at, dz):
        wide = source.astype(F32)
        normed = (
            wide * lax.rsqrt(jnp.mean(wide * wide, axis=-1, keepdims=True) + EPS) * gain_ref[...]
        ).astype(BF16)
        out = lax.dot_general(
            normed, w_all[...], (((1,), (1,)), ((), ())), preferred_element_type=F32
        ).astype(BF16)
        v = out[:, 320:384]
        k = out[:, 256:320].reshape(count // 32, 2, 16, HEAD_DIM)
        here = pl.ds(stage_at, count)
        here_k = pl.ds(stage_at // 2, count // 2)
        for i in range(RING):
            stage_qv[i, here] = jnp.concatenate([out[:, i * 64 : i * 64 + 64], v], axis=1)
        stage_k[here_k] = jnp.concatenate([k[:, 0], k[:, 1]], axis=2).reshape(count // 2, 128)
        nz = lax.rem(z + dz, RING)

        def spot(dy, halved):
            ny = lax.rem(y + dy, RING)
            start = (nz * RING + ny) * rows + first
            if halved:
                return pl.ds(pl.multiple_of(lax.div(start, 2), 16), count // 2)
            return pl.ds(pl.multiple_of(start, 32), count)

        for o in (1, 3, 2):
            ny = lax.rem(y + o, RING)
            go(rcopy(stage_qv.at[ny, here], qv_ref.at[spot(0, False)], a_s.at[n, o], a_r.at[n, o], at(dy=o)))
            go(rcopy(stage_k.at[here_k], kk_ref.at[spot(0, True)], b_s.at[n, o], b_r.at[n, o], at(dy=o)))
        qv_ref[spot(0, False)] = stage_qv[y, here]
        kk_ref[spot(0, True)] = stage_k[here_k]
        waits = []
        for o in (1, 3, 2):
            s, t = qv_ref.at[spot(RING - o, False)], kk_ref.at[spot(RING - o, True)]
            waits.append(rcopy(s, s, a_s.at[n, o], a_r.at[n, o], at(dy=o)))
            waits.append(rcopy(t, t, b_s.at[n, o], b_r.at[n, o], at(dy=o)))
        return waits

    with jax.named_scope("chunk012"):
        pending = chunk(0, x_ref[...], 0, rows, 0, 0)
        pending += chunk(1, xg[0, lo], 0, half, rows, 3)
        pending += chunk(2, xg[1, hi], half, half, rows + half, 1)
    with jax.named_scope("wait_oy"):
        for d in (0, 1):
            oy(d, True).wait_recv()
            go(oy_far(d, back(d)))
        for o in (1, 3):
            for d in (0, 1):
                go(ox(o, d, False))
    with jax.named_scope("wait_oyfar"):
        for d in (0, 1):
            oy_far(d, 2).wait_recv()
        for d in (0, 1):
            go(ox(2, d, False))
        go(oc(0, False))
    with jax.named_scope("wait_x1"):
        x_in(0, 1).wait_recv()
        pending += chunk(3, xg[0, hi], half, half, 2 * rows, 3)
        x_in(1, 1).wait_recv()
        pending += chunk(4, xg[1, lo], 0, half, 2 * rows + half, 1)
    with jax.named_scope("wait_ox"):
        for o in (0, 1, 3):
            for d in (0, 1):
                ox(o, d, True).wait_recv()
                go(ox_far(o, d, back(d)))
    n, place = 5, 3 * rows
    for i in (0, 1):
        a, count = cuts[i]
        for d in (0, 1):
            with jax.named_scope("wait_far%d%d" % (i, d)):
                far_z(d, i, True).wait_recv()
                first = a + (0 if d == 0 else half)
                pending += chunk(n, xg[2, pl.ds(first, count)], first, count, place, 2)
                n, place = n + 1, place + count
        if i == 0:
            with jax.named_scope("wait_ox2"):
                for d in (0, 1):
                    ox(2, d, True).wait_recv()
                    go(ox_far(2, d, back(d)))
                go(oc(3, False))
                go(oc(1, False))
    with jax.named_scope("wait_oxfar"):
        for o in (0, 1, 3, 2):
            for d in (0, 1):
                ox_far(o, d, 2).wait_recv()
        go(oc(2, False))
    with jax.named_scope("wait_qkv"):
        for w in pending:
            w.wait_recv()
    with jax.named_scope("wait_oc"):
        for dx in (0, 3, 1, 2):
            oc(dx, True).wait_recv()
    with jax.named_scope("wait_send"):
        for s in sent:
            s.wait_send()


def project(x, gain, wq, wk, wv, wo):
    rows, width = x.shape
    length = rows * RING * RING
    depth = wq.shape[1]
    dma = pltpu.SemaphoreType.DMA
    vmem = pl.BlockSpec(memory_space=pltpu.VMEM)
    return pl.pallas_call(
        project_kernel,
        name="project",
        out_shape=(
            jax.ShapeDtypeStruct((length, 128), BF16),
            jax.ShapeDtypeStruct((length // 2, 128), BF16),
            jax.ShapeDtypeStruct((RING, RING, wo.shape[0], wo.shape[1] * 2 * RING), BF16),
        ),
        in_specs=[vmem] * 6,
        out_specs=(vmem, vmem, vmem),
        scratch_shapes=[
            pltpu.VMEM((2, RING, RING, 96, depth), BF16),
            pltpu.VMEM((384, width), BF16),
            pltpu.VMEM((3, rows, width), BF16),
            pltpu.VMEM((RING, RING * rows, 128), BF16),
            pltpu.VMEM((RING * rows // 2, 128), BF16),
            dma((4,)), dma((4,)), dma((2, 4)), dma((2, 4)), dma((2, 4)), dma((2, 4)), dma((4,)), dma((4,)),
            dma((2, 2)), dma((2, 2)), dma((2, 2)), dma((2, 2)),
            dma((9, 4)), dma((9, 4)), dma((9, 4)), dma((9, 4)),
            dma((2, 2)), dma((2, 2)), dma((2, 2)), dma((2, 2)), dma((2, 4)), dma((2, 4)),
            dma((2, 4)), dma((2, 4)), dma((4,)), dma((4,)), dma(()),
        ],
        compiler_params=pltpu.CompilerParams(
            collective_id=0, has_side_effects=True, vmem_limit_bytes=48 << 20
        ),
    )(x, gain, wq, wk, wv, wo)


BLOCK_Q = 768
BLOCK_K = 256


def attend_kernel(
    qv_ref, kk_ref, b_ref, g_ref, ho_ref, keys_t, qa, vv, tri, acc, car, stage, h_s, h_r
):
    length = qv_ref.shape[0]
    rows_each = length // (RING * RING)
    z, y, x, c, at = places()
    me = z * RING + y
    barrier = pltpu.get_barrier_semaphore()
    for dz in range(RING):
        for dy in range(RING):
            if dz or dy:
                pl.semaphore_signal(barrier, inc=1, device_id=at(dz=dz, dy=dy), device_id_type=MESH)
    r = lax.broadcasted_iota(jnp.int32, (BLOCK_K, BLOCK_K), 0)
    c = lax.broadcasted_iota(jnp.int32, (BLOCK_K, BLOCK_K), 1)
    tri[...] = jnp.where(r > c, 1.0, 0.0).astype(BF16)
    step = 512

    @pl.loop(0, length // step)
    def _(i):
        rows = pl.ds(pl.multiple_of(i * step, step), step)
        packed = kk_ref[pl.ds(pl.multiple_of(i * (step // 2), step // 2), step // 2), :]
        packed = packed.reshape(step // 32, 16, 128)
        k = jnp.concatenate([packed[:, :, 0:64], packed[:, :, 64:128]], axis=1).reshape(step, HEAD_DIM)
        kk = k.astype(F32) * (LOG2E / 8.0)
        hi = kk.astype(BF16)
        lo = (kk - hi.astype(F32)).astype(BF16)
        keys_t[0:128, rows] = jnp.concatenate([hi, lo], axis=1).T
        bb = b_ref[0:1, rows] * LOG2E
        bh = bb.astype(BF16)
        r1 = bb - bh.astype(F32)
        bm = r1.astype(BF16)
        bl = (r1 - bm.astype(F32)).astype(BF16)
        keys_t[128:144, rows] = jnp.concatenate([bh, bm, bl, jnp.zeros((13, step), BF16)], axis=0)
        both = qv_ref[rows, :]
        qq = both[:, 0:64]
        lane = lax.broadcasted_iota(jnp.int32, (step, 128), 1)
        qa[rows, 0:128] = jnp.concatenate([qq, qq], axis=1)
        qa[rows, 128:256] = jnp.where(lane < 3, 1.0, 0.0).astype(BF16)
        vv[rows, :] = both[:, 64:128]

    pl.semaphore_wait(barrier, RING * RING - 1)
    ratio = BLOCK_Q // BLOCK_K

    @pl.loop(0, length // BLOCK_Q)
    def _(i):
        rows = pl.ds(pl.multiple_of(i * BLOCK_Q, BLOCK_Q), BLOCK_Q)
        q = qa[rows, 0:144]

        def one(q, j, carry, diagonal=False):
            count = q.shape[0]
            cols = pl.ds(pl.multiple_of(j * BLOCK_K, BLOCK_K), BLOCK_K)
            l2 = jnp.dot(q, keys_t[:, cols], preferred_element_type=F32)
            if diagonal:
                t = lax.broadcasted_iota(jnp.int32, (BLOCK_K, BLOCK_K), 0)
                s = lax.broadcasted_iota(jnp.int32, (BLOCK_K, BLOCK_K), 1)
                first = jnp.where(s < t, l2[0:BLOCK_K], -1e30)
                l2 = first if count == BLOCK_K else jnp.concatenate([first, l2[BLOCK_K:]], axis=0)
            mx = jnp.maximum(l2, 0.0)
            mn = jnp.minimum(l2, 0.0)
            log_part = jnp.log2(1.0 + jnp.exp2(mn - mx))
            drop = (mx + log_part).astype(BF16)
            after = jnp.dot(drop, tri[...], preferred_element_type=F32)
            x = (mn - log_part) - after - jnp.concatenate([carry] * (BLOCK_K // 128), axis=1)
            sticks = jnp.exp2(x).astype(BF16)
            pv = jnp.dot(sticks, vv[cols, :], preferred_element_type=F32)
            whole = after[:, 0:1] + drop[:, 0:128].astype(F32)[:, 0:1]
            return pv, carry + jnp.broadcast_to(whole, carry.shape)

        carry = None
        total = None
        for d in reversed(range(ratio)):
            fresh = jnp.zeros((BLOCK_K, 128), F32)
            carry = fresh if carry is None else jnp.concatenate([fresh, carry], axis=0)
            pv, carry = one(q[d * BLOCK_K :], i * ratio + d, carry, True)
            if total is None:
                total = pv
            else:
                total = jnp.concatenate([pv[:BLOCK_K], pv[BLOCK_K:] + total], axis=0)
        acc[...] = total
        car[...] = carry

        def several(n, _):
            base = i * ratio - 1 - n * ratio
            cc, a = car[...], acc[...]
            for u in range(ratio):
                pv, cc = one(q, base - u, cc)
                a = a + pv
            acc[...] = a
            car[...] = cc
            return 0

        lax.fori_loop(0, i, several, 0)
        a = acc[...]
        scaled = a * lax.rsqrt(jnp.mean(a * a, axis=-1, keepdims=True) + EPS)
        head = (scaled * g_ref[...]).astype(BF16)
        for yy in range(RING):
            part = head[yy * rows_each : (yy + 1) * rows_each]
            half = rows_each // 2
            stage[i * RING + yy] = jnp.concatenate([part[:half], part[half:]], axis=1)
        for yy in range(RING):
            dest = i * RING + yy

            @pl.when(dest != me)
            def _():
                rcopy(
                    stage.at[dest], ho_ref.at[y * RING + z], h_s.at[dest], h_r.at[me],
                    {"sp": dest, "dp": lax.axis_index("dp")},
                ).start()

            @pl.when(dest == me)
            def _():
                ho_ref[y * RING + z] = stage[dest]

    for dz in range(RING):
        for dy in range(RING):
            if dz or dy:
                nz, ny = lax.rem(z + dz, RING), lax.rem(y + dy, RING)
                other = nz * RING + ny
                slot = ho_ref.at[ny * RING + nz]
                w = rcopy(slot, slot, h_s.at[other], h_r.at[other], at(dz=dz, dy=dy))
                w.wait_recv()
                w.wait_send()


def attend(qv, kk, bias, gain):
    length = qv.shape[0]
    each = length // (RING * RING)
    vmem = pl.BlockSpec(memory_space=pltpu.VMEM)
    dma = pltpu.SemaphoreType.DMA
    return pl.pallas_call(
        attend_kernel,
        name="attend",
        out_shape=jax.ShapeDtypeStruct((RING * RING, each // 2, 2 * HEAD_DIM), BF16),
        in_specs=[vmem] * 4,
        out_specs=vmem,
        scratch_shapes=[
            pltpu.VMEM((144, length), BF16),
            pltpu.VMEM((length, 256), BF16),
            pltpu.VMEM((length, HEAD_DIM), BF16),
            pltpu.VMEM((BLOCK_K, BLOCK_K), BF16),
            pltpu.VMEM((BLOCK_Q, HEAD_DIM), F32),
            pltpu.VMEM((BLOCK_Q, 128), F32),
            pltpu.VMEM((RING * RING, each // 2, 2 * HEAD_DIM), BF16),
            dma((RING * RING,)), dma((RING * RING,)),
        ],
        compiler_params=pltpu.CompilerParams(
            collective_id=1, has_side_effects=True, vmem_limit_bytes=48 << 20
        ),
    )(qv, kk, bias, gain)


def mix_kernel(ho_ref, wo_ref, o_ref, lhs):
    heads, half, _ = ho_ref.shape
    for n in range(0, heads, 2):
        a, b = ho_ref[n], ho_ref[n + 1]
        cols = pl.ds(n * HEAD_DIM, 2 * HEAD_DIM)
        lhs[0:half, cols] = jnp.concatenate([a[:, 0:64], b[:, 0:64]], axis=1)
        lhs[half : 2 * half, cols] = jnp.concatenate([a[:, 64:128], b[:, 64:128]], axis=1)
    width = o_ref.shape[1]
    for n in range(0, width, 512):
        o_ref[:, n : n + 512] = jnp.dot(
            lhs[...], wo_ref[:, n : n + 512], preferred_element_type=F32
        ).astype(BF16)


def mix(ho, wo):
    heads, half, _ = ho.shape
    vmem = pl.BlockSpec(memory_space=pltpu.VMEM)
    return pl.pallas_call(
        mix_kernel,
        name="mix",
        out_shape=jax.ShapeDtypeStruct((2 * half, wo.shape[1]), BF16),
        in_specs=[vmem] * 2,
        out_specs=vmem,
        scratch_shapes=[pltpu.VMEM((2 * half, heads * HEAD_DIM), BF16)],
        compiler_params=pltpu.CompilerParams(vmem_limit_bytes=48 << 20),
    )(ho, wo)


def body(inputs, in_gain, w_query, w_key, w_value, key_bias, out_gain, w_out):
    own = lax.axis_index("sp")
    qv, kk, wo = project(inputs[0], in_gain[None], w_query.T, w_key.T, w_value.T, w_out)
    gain = lax.dynamic_slice_in_dim(out_gain, own * HEAD_DIM, HEAD_DIM, 0)[None]
    ho = attend(qv, kk, key_bias[0].T, gain)
    return mix(ho, wo.reshape(-1, wo.shape[-1]))[None]


def solution(mesh):
    placed = (
        P("dp", "sp", None), P(), P("dp", "sp"), P("dp", "sp"), P("dp", "sp"),
        P("dp", None, "sp"), P(), P("sp", "dp"),
    )
    return jax.shard_map(body, mesh=mesh, in_specs=placed, out_specs=P("dp", "sp", None), check_vma=False)
```

time: 120 us -> 90.1 us (0.75)
  the two profiles are of different devices: /device:TPU:0 before, /device:TPU:96 now
where the time goes in v2:
time: 90.1 us; the launch traced here: 89.1 us
  Pallas kernels  80.7 us (90%)
  local copies, waits for them, and re-layouts  8.38 us (9%)
    pallas_call x1, Pallas kernels, project(): pl.pallas_call(project_kernel, name='project', out_shape=(jax.ShapeDtypeS...  53 us
    pallas_call x1, Pallas kernels, attend(): pl.pallas_call(attend_kernel, name='attend', out_shape=jax.ShapeDtypeStru...  25.8 us
    unnamed x18, local copies, waits for them, and re-layouts  8.31 us
    pallas_call x1, Pallas kernels, mix(): pl.pallas_call(mix_kernel, name='mix', out_shape=jax.ShapeDtypeStruct((2...  1.92 us

profile of v2, /device:TPU:96, one launch (start us, length us, event | category | flops | bytes accessed | tf_op | source)
XLA Modules:
  0.0 89.1 jit_solution(14751763663748591051)
XLA Ops:
  0.0 0.0 copy-start
  0.0 0.7 copy-done
  0.7 0.1 dynamic-slice_bitcast_fusion.g_ref
  0.8 0.0 copy-start.2
  0.8 1.1 %copy-done.2 = bf16[1,192,2048]{2,1,0:T(8,128)(2,1)S(1)} copy-done((bf16[1,192,2048]{2,1,0:T(8,128)(2,1)S(1)}, bf16[1,192,2048]{2,1,0:T(8,128)(2,1)}, u32[]{:S(2)}) %copy-start.2) | copy-done | bytes 786456
  1.9 0.0 copy-start.3
  1.9 0.8 copy-done.3
  2.7 0.0 copy-start.4
  2.7 0.8 copy-done.4
  3.4 0.0 copy-start.6
  3.4 0.7 copy-done.6
  4.1 0.0 copy-start.7
  4.1 0.7 copy-done.7
  4.8 0.0 copy-start.8
  4.8 0.7 copy-done.8
  5.5 53.0 %project.1 = (bf16[3072,128]{1,0:T(8,128)(2,1)S(1)}, bf16[1536,128]{1,0:T(8,128)(2,1)S(1)}, bf16[4,4,64,2048]{3,2,1,0:T(8,128)(2,1)}) custom-call(bf16[192,2048]{1,0:T(8,128)(2,1)S(1)} %bitcast.11, f32[1,2048]{1,0:T(1,128)S(1)} %bitcast.14, bf16[64,256]{1,0:T(8,128)(2,1)S(1)} %bitcast.12, bf16[16,256]{1,0:T(8,128)(2,1)S(1)} %bitcast.15, ...), custom_call_target="tpu_custom_call" | custom-call | tf_op jit(solution)/shard_map/project/pallas_call | solution.py:306
  58.5 0.0 copy-start.5
  58.5 0.7 copy-done.5
  59.2 25.8 %attend.1.ho_ref = bf16[16,96,128]{2,1,0:T(8,128)(2,1)S(1)} custom-call(bf16[3072,128]{1,0:T(8,128)(2,1)S(1)} %get-tuple-element.8.qv_ref, bf16[1536,128]{1,0:T(8,128)(2,1)S(1)} %get-tuple-element.9.kk_ref, f32[1,3072]{1,0:T(1,128)S(1)} %bitcast.13, f32[1,64]{1,0:T(1,128)S(1)} %dynamic-slice_bitcast_fusion.g_ref), custom_call_target="tpu_custom_call" | custom-call | tf_op jit(solution)/shard_map/attend/pallas_call | solution.py:467
  85.0 0.0 copy-start.1
  85.0 2.2 %copy-done.1 = bf16[4,4,64,2048]{3,2,1,0:T(8,128)(2,1)S(1)} copy-done((bf16[4,4,64,2048]{3,2,1,0:T(8,128)(2,1)S(1)}, bf16[4,4,64,2048]{3,2,1,0:T(8,128)(2,1)}, u32[]{:S(2)}) %copy-start.1) | copy-done | bytes 4194328
  87.2 1.9 %mix.1 = bf16[192,2048]{1,0:T(8,128)(2,1)} custom-call(bf16[16,96,128]{2,1,0:T(8,128)(2,1)S(1)} %attend.1.ho_ref, bf16[1024,2048]{1,0:T(8,128)(2,1)S(1)} %bitcast.10), custom_call_target="tpu_custom_call" | custom-call | tf_op jit(solution)/shard_map/mix/pallas_call | solution.py:506
Async XLA Ops:
  0.0 0.7 copy-start
  0.8 1.1 %copy-start.2 = (bf16[1,192,2048]{2,1,0:T(8,128)(2,1)S(1)}, bf16[1,192,2048]{2,1,0:T(8,128)(2,1)}, u32[]{:S(2)}) copy-start(bf16[1,192,2048]{2,1,0:T(8,128)(2,1)} %param.8) | copy-start | bytes 2359300
  1.9 0.8 copy-start.3
  2.7 0.8 copy-start.4
  3.4 0.7 copy-start.6
  4.1 0.7 copy-start.7
  4.8 0.7 copy-start.8
  58.5 0.7 copy-start.5
  85.0 2.2 %copy-start.1 = (bf16[4,4,64,2048]{3,2,1,0:T(8,128)(2,1)S(1)}, bf16[4,4,64,2048]{3,2,1,0:T(8,128)(2,1)}, u32[]{:S(2)}) copy-start(bf16[4,4,64,2048]{3,2,1,0:T(8,128)(2,1)} %get-tuple-element.10) | copy-start | bytes 12582916

commit v3 on v2

--- a/solution.py
+++ b/solution.py
@@ -36,29 +36,42 @@
 
 
 def project_kernel(
-    x_ref, gain_ref, wq_ref, wk_ref, wv_ref, wo_in,
+    x_hbm, gain_hbm, wq_hbm, wk_hbm, wv_hbm, wo_hbm,
     qv_ref, kk_ref, wo_ref,
     packs, w_all, xg, stage_qv, stage_k,
     wy_s, wy_r, wx_s, wx_r, wf_s, wf_r, wc_s, wc_r, xd_s, xd_r, xf_s, xf_r, a_s, a_r, b_s, b_r,
     oz_s, oz_r, oy_s, oy_r, ox_s, ox_r, of_s, of_r, oc_s, oc_r, local_sem,
+    x_ref, gain_ref, wq_ref, wk_ref, wv_ref, wo_in,
 ):
     z, y, x, c, at = places()
+    loads = [
+        pltpu.make_async_copy(s, d, local_sem.at[i])
+        for i, (s, d) in enumerate(
+            (
+                (wq_hbm, wq_ref), (wk_hbm, wk_ref), (wv_hbm, wv_ref), (wo_hbm, wo_in),
+                (gain_hbm, gain_ref), (x_hbm, x_ref),
+            )
+        )
+    ]
+    for load in loads:
+        load.start()
+    friends = [at(dz=1), at(dz=2), at(dz=3), at(dy=1), at(dy=2), at(dy=3), at(dx=1), at(dx=3), at(dc=1)]
+    barrier = pltpu.get_barrier_semaphore()
+    for f in friends:
+        pl.semaphore_signal(barrier, inc=1, device_id=f, device_id_type=MESH)
+    for load in loads:
+        load.wait()
     rows = x_ref.shape[0]
     half = rows // 2
     depth = wq_ref.shape[1]
     qn, kn = wq_ref.shape[0], wk_ref.shape[0]
     piece_rows = qn + 2 * kn
     packs[c, x, y] = jnp.concatenate([wq_ref[...], wk_ref[...], wv_ref[...]], axis=0)
-    friends = [at(dz=1), at(dz=3), at(dy=1), at(dy=2), at(dy=3), at(dx=1), at(dx=3), at(dc=1)]
-    barrier = pltpu.get_barrier_semaphore()
-    for f in friends:
-        pl.semaphore_signal(barrier, inc=1, device_id=f, device_id_type=MESH)
 
     def wo_cols(dx, cc):
         return pl.ds(pl.multiple_of((lax.rem(x + dx, RING) * 2 + cc) * depth, depth), depth)
 
-    own_wo = pltpu.make_async_copy(wo_in, wo_ref.at[y, z, :, wo_cols(0, c)], local_sem)
-    own_wo.start()
+    wo_ref[y, z, :, wo_cols(0, c)] = wo_in[...]
     pl.semaphore_wait(barrier, len(friends))
 
     sent = []
@@ -79,16 +92,14 @@
     def oz(dz, n):
         return wo_ref.at[y, lax.rem(z + dz, RING), n, wo_cols(0, c)]
 
-    every, top, low = pl.ds(0, 64), pl.ds(0, 32), pl.ds(32, 32)
-    go_oz = [rcopy(wo_in, oz(0, every), oz_s.at[d, 0], oz_r.at[d, 0], near(d, "dz")) for d in (0, 1)]
-
-    def oz_in(d):
-        s = oz(back(d), every)
-        return rcopy(s, s, oz_s.at[d, 0], oz_r.at[d, 0], near(d, "dz"))
-
-    def oz_far(d, dz):
-        s = oz(dz, top if d == 0 else low)
-        return rcopy(s, s, oz_s.at[d, 1], oz_r.at[d, 1], near(d, "dz"))
+    every = slice(None)
+
+    def oz_out(dz):
+        return rcopy(wo_in, oz(0, every), oz_s.at[dz], oz_r.at[dz], at(dz=dz))
+
+    def oz_in(dz):
+        s = oz(RING - dz, every)
+        return rcopy(s, s, oz_s.at[dz], oz_r.at[dz], at(dz=dz))
 
     def x_out(d, i):
         p = halves[i if d == 0 else 1 - i]
@@ -149,8 +160,8 @@
             go(w_y(o, False))
         for d in (0, 1):
             go(w_x(0, d, False))
-        for d in (0, 1):
-            go(go_oz[d])
+        for dz in (2, 1, 3):
+            go(oz_out(dz))
         for i in (0, 1):
             for d in (0, 1):
                 go(x_out(d, i))
@@ -161,10 +172,10 @@
                 go(w_x(o, d, False))
         go(w_c(0, False))
     with jax.named_scope("wait_oz"):
-        own_wo.wait()
-        for d in (0, 1):
-            oz_in(d).wait_recv()
-            go(oz_far(d, back(d)))
+        for dz in (1, 3, 2):
+            oz_in(dz).wait_recv()
+        for d in (0, 1):
+            go(oy(d, False))
     with jax.named_scope("wait_wx"):
         for o in (0, 1, 3, 2):
             for d in (0, 1):
@@ -172,12 +183,15 @@
                 go(w_far(o, d, back(d)))
         go(w_c(3, False))
         go(w_c(1, False))
-    with jax.named_scope("wait_ozfar"):
-        for d in (0, 1):
-            oz_far(d, 2).wait_recv()
-        for d in (0, 1):
-            go(oy(d, False))
+        for d in (0, 1):
             go(ox(0, d, False))
+    with jax.named_scope("wait_oy"):
+        for d in (0, 1):
+            oy(d, True).wait_recv()
+            go(oy_far(d, back(d)))
+        for o in (1, 3):
+            for d in (0, 1):
+                go(ox(o, d, False))
     with jax.named_scope("wait_wfar"):
         for o in (0, 1, 3, 2):
             for d in (0, 1):
@@ -188,99 +202,97 @@
             x_in(d, 0).wait_recv()
             for i in (0, 1):
                 go(far_z(d, i, False))
+    with jax.named_scope("wait_oyfar"):
+        for d in (0, 1):
+            oy_far(d, 2).wait_recv()
+        for d in (0, 1):
+            go(ox(2, d, False))
+        go(oc(0, False))
     with jax.named_scope("wait_wc"):
         for dx in (0, 3, 1, 2):
             w_c(dx, True).wait_recv()
 
     with jax.named_scope("assemble"):
         for n in range(2 * RING):
-            cols = pl.ds(n * depth, depth)
-            for i in range(RING):
-                p = packs[n % 2, n // 2, i]
-                w_all[i * qn : (i + 1) * qn, cols] = p[0:qn]
-                w_all[RING * qn + i * kn : RING * qn + (i + 1) * kn, cols] = p[qn : qn + kn]
-                w_all[RING * (qn + kn) + i * kn : RING * (qn + kn) + (i + 1) * kn, cols] = p[qn + kn :]
-
-    def chunk(n, source, first, count, stage_at, dz):
+            p = [packs[n % 2, n // 2, i] for i in range(RING)]
+            w_all[n * depth : (n + 1) * depth, :] = jnp.concatenate(
+                [t[0:qn] for t in p] + [t[qn : qn + kn] for t in p] + [t[qn + kn :] for t in p], axis=0
+            ).T
+
+    def chunk(n, source, segments, stage_at):
         wide = source.astype(F32)
         normed = (
             wide * lax.rsqrt(jnp.mean(wide * wide, axis=-1, keepdims=True) + EPS) * gain_ref[...]
         ).astype(BF16)
-        out = lax.dot_general(
-            normed, w_all[...], (((1,), (1,)), ((), ())), preferred_element_type=F32
-        ).astype(BF16)
+        out = jnp.dot(normed, w_all[...], preferred_element_type=F32).astype(BF16)
+        total = out.shape[0]
         v = out[:, 320:384]
-        k = out[:, 256:320].reshape(count // 32, 2, 16, HEAD_DIM)
-        here = pl.ds(stage_at, count)
-        here_k = pl.ds(stage_at // 2, count // 2)
+        k = out[:, 256:320].reshape(total // 32, 2, 16, HEAD_DIM)
         for i in range(RING):
-            stage_qv[i, here] = jnp.concatenate([out[:, i * 64 : i * 64 + 64], v], axis=1)
-        stage_k[here_k] = jnp.concatenate([k[:, 0], k[:, 1]], axis=2).reshape(count // 2, 128)
-        nz = lax.rem(z + dz, RING)
-
-        def spot(dy, halved):
-            ny = lax.rem(y + dy, RING)
-            start = (nz * RING + ny) * rows + first
-            if halved:
-                return pl.ds(pl.multiple_of(lax.div(start, 2), 16), count // 2)
-            return pl.ds(pl.multiple_of(start, 32), count)
-
-        for o in (1, 3, 2):
-            ny = lax.rem(y + o, RING)
-            go(rcopy(stage_qv.at[ny, here], qv_ref.at[spot(0, False)], a_s.at[n, o], a_r.at[n, o], at(dy=o)))
-            go(rcopy(stage_k.at[here_k], kk_ref.at[spot(0, True)], b_s.at[n, o], b_r.at[n, o], at(dy=o)))
-        qv_ref[spot(0, False)] = stage_qv[y, here]
-        kk_ref[spot(0, True)] = stage_k[here_k]
+            stage_qv[i, pl.ds(stage_at, total)] = jnp.concatenate([out[:, i * 64 : i * 64 + 64], v], axis=1)
+        stage_k[pl.ds(stage_at // 2, total // 2)] = jnp.concatenate([k[:, 0], k[:, 1]], axis=2).reshape(
+            total // 2, 128
+        )
         waits = []
-        for o in (1, 3, 2):
-            s, t = qv_ref.at[spot(RING - o, False)], kk_ref.at[spot(RING - o, True)]
-            waits.append(rcopy(s, s, a_s.at[n, o], a_r.at[n, o], at(dy=o)))
-            waits.append(rcopy(t, t, b_s.at[n, o], b_r.at[n, o], at(dy=o)))
+        for dz, first, count in segments:
+            here, here_k = pl.ds(stage_at, count), pl.ds(stage_at // 2, count // 2)
+            nz = lax.rem(z + dz, RING)
+
+            def spot(dy, halved):
+                start = (nz * RING + lax.rem(y + dy, RING)) * rows + first
+                if halved:
+                    return pl.ds(pl.multiple_of(lax.div(start, 2), 16), count // 2)
+                return pl.ds(pl.multiple_of(start, 32), count)
+
+            for o in (2, 1, 3):
+                ny = lax.rem(y + o, RING)
+                go(rcopy(stage_qv.at[ny, here], qv_ref.at[spot(0, False)], a_s.at[n, o], a_r.at[n, o], at(dy=o)))
+                go(rcopy(stage_k.at[here_k], kk_ref.at[spot(0, True)], b_s.at[n, o], b_r.at[n, o], at(dy=o)))
+            qv_ref[spot(0, False)] = stage_qv[y, here]
+            kk_ref[spot(0, True)] = stage_k[here_k]
+            for o in (1, 3, 2):
+                s, t = qv_ref.at[spot(RING - o, False)], kk_ref.at[spot(RING - o, True)]
+                waits.append(rcopy(s, s, a_s.at[n, o], a_r.at[n, o], at(dy=o)))
+                waits.append(rcopy(t, t, b_s.at[n, o], b_r.at[n, o], at(dy=o)))
+            n, stage_at = n + 1, stage_at + count
         return waits
 
     with jax.named_scope("chunk012"):
-        pending = chunk(0, x_ref[...], 0, rows, 0, 0)
-        pending += chunk(1, xg[0, lo], 0, half, rows, 3)
-        pending += chunk(2, xg[1, hi], half, half, rows + half, 1)
-    with jax.named_scope("wait_oy"):
-        for d in (0, 1):
-            oy(d, True).wait_recv()
-            go(oy_far(d, back(d)))
-        for o in (1, 3):
-            for d in (0, 1):
-                go(ox(o, d, False))
-    with jax.named_scope("wait_oyfar"):
-        for d in (0, 1):
-            oy_far(d, 2).wait_recv()
-        for d in (0, 1):
-            go(ox(2, d, False))
-        go(oc(0, False))
+        pending = chunk(0, x_ref[...], ((0, 0, rows),), 0)
+        pending += chunk(
+            1, jnp.concatenate([xg[0, lo], xg[1, hi]], axis=0), ((3, 0, half), (1, half, half)), rows
+        )
+    with jax.named_scope("wait_ox"):
+        for o in (0, 1, 3):
+            for d in (0, 1):
+                ox(o, d, True).wait_recv()
+                go(ox_far(o, d, back(d)))
     with jax.named_scope("wait_x1"):
         x_in(0, 1).wait_recv()
-        pending += chunk(3, xg[0, hi], half, half, 2 * rows, 3)
         x_in(1, 1).wait_recv()
-        pending += chunk(4, xg[1, lo], 0, half, 2 * rows + half, 1)
-    with jax.named_scope("wait_ox"):
-        for o in (0, 1, 3):
-            for d in (0, 1):
-                ox(o, d, True).wait_recv()
-                go(ox_far(o, d, back(d)))
-    n, place = 5, 3 * rows
+        pending += chunk(
+            3, jnp.concatenate([xg[0, hi], xg[1, lo]], axis=0), ((3, half, half), (1, 0, half)), 2 * rows
+        )
+    with jax.named_scope("wait_ox2"):
+        for d in (0, 1):
+            ox(2, d, True).wait_recv()
+            go(ox_far(2, d, back(d)))
+        go(oc(3, False))
+        go(oc(1, False))
+    place = 3 * rows
     for i in (0, 1):
         a, count = cuts[i]
-        for d in (0, 1):
-            with jax.named_scope("wait_far%d%d" % (i, d)):
+        with jax.named_scope("wait_far%d" % i):
+            for d in (0, 1):
                 far_z(d, i, True).wait_recv()
-                first = a + (0 if d == 0 else half)
-                pending += chunk(n, xg[2, pl.ds(first, count)], first, count, place, 2)
-                n, place = n + 1, place + count
-        if i == 0:
-            with jax.named_scope("wait_ox2"):
-                for d in (0, 1):
-                    ox(2, d, True).wait_recv()
-                    go(ox_far(2, d, back(d)))
-                go(oc(3, False))
-                go(oc(1, False))
+        with jax.named_scope("chunk_far%d" % i):
+            pending += chunk(
+                5 + 2 * i,
+                jnp.concatenate([xg[2, pl.ds(a, count)], xg[2, pl.ds(a + half, count)]], axis=0),
+                ((2, a, count), (2, a + half, count)),
+                place,
+            )
+            place += 2 * count
     with jax.named_scope("wait_oxfar"):
         for o in (0, 1, 3, 2):
             for d in (0, 1):
@@ -311,22 +323,24 @@
             jax.ShapeDtypeStruct((length // 2, 128), BF16),
             jax.ShapeDtypeStruct((RING, RING, wo.shape[0], wo.shape[1] * 2 * RING), BF16),
         ),
-        in_specs=[vmem] * 6,
+        in_specs=[pl.BlockSpec(memory_space=pltpu.HBM)] * 6,
         out_specs=(vmem, vmem, vmem),
         scratch_shapes=[
             pltpu.VMEM((2, RING, RING, 96, depth), BF16),
-            pltpu.VMEM((384, width), BF16),
+            pltpu.VMEM((width, 384), BF16),
             pltpu.VMEM((3, rows, width), BF16),
             pltpu.VMEM((RING, RING * rows, 128), BF16),
             pltpu.VMEM((RING * rows // 2, 128), BF16),
             dma((4,)), dma((4,)), dma((2, 4)), dma((2, 4)), dma((2, 4)), dma((2, 4)), dma((4,)), dma((4,)),
             dma((2, 2)), dma((2, 2)), dma((2, 2)), dma((2, 2)),
             dma((9, 4)), dma((9, 4)), dma((9, 4)), dma((9, 4)),
-            dma((2, 2)), dma((2, 2)), dma((2, 2)), dma((2, 2)), dma((2, 4)), dma((2, 4)),
-            dma((2, 4)), dma((2, 4)), dma((4,)), dma((4,)), dma(()),
+            dma((4,)), dma((4,)), dma((2, 2)), dma((2, 2)), dma((2, 4)), dma((2, 4)),
+            dma((2, 4)), dma((2, 4)), dma((4,)), dma((4,)), dma((6,)),
+            pltpu.VMEM(x.shape, BF16), pltpu.VMEM(gain.shape, F32), pltpu.VMEM(wq.shape, BF16),
+            pltpu.VMEM(wk.shape, BF16), pltpu.VMEM(wv.shape, BF16), pltpu.VMEM(wo.shape, BF16),
         ],
         compiler_params=pltpu.CompilerParams(
-            collective_id=0, has_side_effects=True, vmem_limit_bytes=48 << 20
+            collective_id=0, has_side_effects=True, vmem_limit_bytes=24 << 20
         ),
     )(x, gain, wq, wk, wv, wo)
 
@@ -336,8 +350,15 @@
 
 
 def attend_kernel(
-    qv_ref, kk_ref, b_ref, g_ref, ho_ref, keys_t, qa, vv, tri, acc, car, stage, h_s, h_r
+    qv_ref, kk_ref, b_hbm, g_hbm, ho_ref, keys_t, qa, vv, tri, acc, car, stage, h_s, h_r,
+    b_ref, g_all, local_sem,
 ):
+    loads = [
+        pltpu.make_async_copy(b_hbm, b_ref, local_sem.at[0]),
+        pltpu.make_async_copy(g_hbm, g_all, local_sem.at[1]),
+    ]
+    for load in loads:
+        load.start()
     length = qv_ref.shape[0]
     rows_each = length // (RING * RING)
     z, y, x, c, at = places()
@@ -362,12 +383,6 @@
         hi = kk.astype(BF16)
         lo = (kk - hi.astype(F32)).astype(BF16)
         keys_t[0:128, rows] = jnp.concatenate([hi, lo], axis=1).T
-        bb = b_ref[0:1, rows] * LOG2E
-        bh = bb.astype(BF16)
-        r1 = bb - bh.astype(F32)
-        bm = r1.astype(BF16)
-        bl = (r1 - bm.astype(F32)).astype(BF16)
-        keys_t[128:144, rows] = jnp.concatenate([bh, bm, bl, jnp.zeros((13, step), BF16)], axis=0)
         both = qv_ref[rows, :]
         qq = both[:, 0:64]
         lane = lax.broadcasted_iota(jnp.int32, (step, 128), 1)
@@ -375,6 +390,16 @@
         qa[rows, 128:256] = jnp.where(lane < 3, 1.0, 0.0).astype(BF16)
         vv[rows, :] = both[:, 64:128]
 
+    for load in loads:
+        load.wait()
+    bb = b_ref[...] * LOG2E
+    bh = bb.astype(BF16)
+    r1 = bb - bh.astype(F32)
+    bm = r1.astype(BF16)
+    bl = (r1 - bm.astype(F32)).astype(BF16)
+    keys_t[128:144, :] = jnp.concatenate([bh, bm, bl, jnp.zeros((13, length), BF16)], axis=0)
+    pair = g_all[0:1, pl.ds(pl.multiple_of(lax.div(me, 2) * 128, 128), 128)]
+    gain = jnp.where(lax.rem(me, 2) == 0, pair[:, 0:64], pair[:, 64:128])
     pl.semaphore_wait(barrier, RING * RING - 1)
     ratio = BLOCK_Q // BLOCK_K
 
@@ -429,7 +454,7 @@
         lax.fori_loop(0, i, several, 0)
         a = acc[...]
         scaled = a * lax.rsqrt(jnp.mean(a * a, axis=-1, keepdims=True) + EPS)
-        head = (scaled * g_ref[...]).astype(BF16)
+        head = (scaled * gain).astype(BF16)
         for yy in range(RING):
             part = head[yy * rows_each : (yy + 1) * rows_each]
             half = rows_each // 2
@@ -468,7 +493,7 @@
         attend_kernel,
         name="attend",
         out_shape=jax.ShapeDtypeStruct((RING * RING, each // 2, 2 * HEAD_DIM), BF16),
-        in_specs=[vmem] * 4,
+        in_specs=[vmem] * 2 + [pl.BlockSpec(memory_space=pltpu.HBM)] * 2,
         out_specs=vmem,
         scratch_shapes=[
             pltpu.VMEM((144, length), BF16),
@@ -479,9 +504,10 @@
             pltpu.VMEM((BLOCK_Q, 128), F32),
             pltpu.VMEM((RING * RING, each // 2, 2 * HEAD_DIM), BF16),
             dma((RING * RING,)), dma((RING * RING,)),
+            pltpu.VMEM(bias.shape, F32), pltpu.VMEM(gain.shape, F32), dma((2,)),
         ],
         compiler_params=pltpu.CompilerParams(
-            collective_id=1, has_side_effects=True, vmem_limit_bytes=48 << 20
+            collective_id=1, has_side_effects=True, vmem_limit_bytes=24 << 20
         ),
     )(qv, kk, bias, gain)
 
@@ -510,15 +536,13 @@
         in_specs=[vmem] * 2,
         out_specs=vmem,
         scratch_shapes=[pltpu.VMEM((2 * half, heads * HEAD_DIM), BF16)],
-        compiler_params=pltpu.CompilerParams(vmem_limit_bytes=48 << 20),
+        compiler_params=pltpu.CompilerParams(vmem_limit_bytes=16 << 20),
     )(ho, wo)
 
 
 def body(inputs, in_gain, w_query, w_key, w_value, key_bias, out_gain, w_out):
-    own = lax.axis_index("sp")
     qv, kk, wo = project(inputs[0], in_gain[None], w_query.T, w_key.T, w_value.T, w_out)
-    gain = lax.dynamic_slice_in_dim(out_gain, own * HEAD_DIM, HEAD_DIM, 0)[None]
-    ho = attend(qv, kk, key_bias[0].T, gain)
+    ho = attend(qv, kk, key_bias[0].T, out_gain[None])
     return mix(ho, wo.reshape(-1, wo.shape[-1]))[None]
 
 

time: 90.1 us -> 72.4 us (0.80)
  Pallas kernels: 80.7 us -> 65.8 us
  local copies, waits for them, and re-layouts: 8.38 us -> 6.12 us
    pallas_call x1, Pallas kernels: 53 us -> 38.8 us  [project(): pl.pallas_call(project_kernel, name='project', out_shape=(jax.ShapeDtypeS...]
    unnamed x18 -> x16, local copies, waits for them, and re-layouts: 8.31 us -> 6.12 us
where the time goes in v3:
time: 72.4 us; the launch traced here: 72 us
  Pallas kernels  65.8 us (91%)
  local copies, waits for them, and re-layouts  6.12 us (8%)
    pallas_call x1, Pallas kernels, project(): pl.pallas_call(project_kernel, name='project', out_shape=(jax.ShapeDtypeS...  38.8 us
    pallas_call x1, Pallas kernels, attend(): pl.pallas_call(attend_kernel, name='attend', out_shape=jax.ShapeDtypeStru...  25.1 us
    unnamed x16, local copies, waits for them, and re-layouts  6.12 us
    pallas_call x1, Pallas kernels, mix(): pl.pallas_call(mix_kernel, name='mix', out_shape=jax.ShapeDtypeStruct((2...  1.96 us

profile of v3, /device:TPU:96, one launch (start us, length us, event | category | flops | bytes accessed | tf_op | source)
XLA Modules:
  0.0 72.0 jit_solution(7809841658804896606)
XLA Ops:
  0.0 0.0 copy-start
  0.0 1.1 %copy-done = bf16[1,192,2048]{2,1,0:T(8,128)(2,1)S(1)} copy-done((bf16[1,192,2048]{2,1,0:T(8,128)(2,1)S(1)}, bf16[1,192,2048]{2,1,0:T(8,128)(2,1)}, u32[]{:S(2)}) %copy-start) | copy-done | bytes 786456
  1.1 0.0 copy-start.1
  1.1 0.8 %copy-done.1 = bf16[256,64]{0,1:T(8,128)(2,1)S(1)} copy-done((bf16[256,64]{0,1:T(8,128)(2,1)S(1)}, bf16[256,64]{0,1:T(8,128)(2,1)}, u32[]{:S(2)}) %copy-start.1) | copy-done | bytes 32792
  1.9 0.0 copy-start.2
  1.9 0.8 %copy-done.2 = bf16[64,256]{1,0:T(8,128)(2,1)S(1)} copy-done((bf16[64,256]{1,0:T(8,128)(2,1)S(1)}, bf16[64,256]{1,0:T(8,128)(2,1)}, u32[]{:S(2)}) %copy-start.2) | copy-done | bytes 32792
  2.7 0.0 copy-start.4
  2.7 0.7 copy-done.4
  3.3 0.0 copy-start.5
  3.4 0.7 copy-done.5
  4.0 0.0 copy-start.6
  4.0 0.7 copy-done.6
  4.7 38.8 %project.1 = (bf16[3072,128]{1,0:T(8,128)(2,1)S(1)}, bf16[1536,128]{1,0:T(8,128)(2,1)S(1)}, bf16[4,4,64,2048]{3,2,1,0:T(8,128)(2,1)S(1)}) custom-call(bf16[192,2048]{1,0:T(8,128)(2,1)S(1)} %bitcast.10, f32[1,2048]{1,0:T(1,128)S(1)} %bitcast.13, bf16[64,256]{1,0:T(8,128)(2,1)S(1)} %bitcast.11, bf16[16,256]{1,0:T(8,128)(2,1)S(1)} %bitcast.14, ...), custom_call_target="tpu_custom_call" | custom-call | tf_op jit(solution)/shard_map/project/pallas_call | solution.py:318
  43.5 0.0 copy-start.3
  43.5 0.7 copy-done.3
  44.2 0.0 copy-start.7
  44.2 0.7 copy-done.7
  44.9 25.1 %attend.1.ho_ref = bf16[16,96,128]{2,1,0:T(8,128)(2,1)S(1)} custom-call(bf16[3072,128]{1,0:T(8,128)(2,1)S(1)} %get-tuple-element.8.qv_ref, bf16[1536,128]{1,0:T(8,128)(2,1)S(1)} %get-tuple-element.9.kk_ref, f32[1,3072]{1,0:T(1,128)S(1)} %bitcast.12, f32[1,1024]{1,0:T(1,128)S(1)} %bitcast.16), custom_call_target="tpu_custom_call" | custom-call | tf_op jit(solution)/shard_map/attend/pallas_call | solution.py:492
  70.0 2.0 %mix.1 = bf16[192,2048]{1,0:T(8,128)(2,1)} custom-call(bf16[16,96,128]{2,1,0:T(8,128)(2,1)S(1)} %attend.1.ho_ref, bf16[1024,2048]{1,0:T(8,128)(2,1)S(1)} %bitcast.9), custom_call_target="tpu_custom_call" | custom-call | tf_op jit(solution)/shard_map/mix/pallas_call | solution.py:532
Async XLA Ops:
  0.0 1.1 %copy-start = (bf16[1,192,2048]{2,1,0:T(8,128)(2,1)S(1)}, bf16[1,192,2048]{2,1,0:T(8,128)(2,1)}, u32[]{:S(2)}) copy-start(bf16[1,192,2048]{2,1,0:T(8,128)(2,1)} %param.8) | copy-start | bytes 2359300
  1.1 0.8 %copy-start.1 = (bf16[256,64]{0,1:T(8,128)(2,1)S(1)}, bf16[256,64]{0,1:T(8,128)(2,1)}, u32[]{:S(2)}) copy-start(bf16[256,64]{0,1:T(8,128)(2,1)} %param.10) | copy-start | bytes 98308
  1.9 0.8 %copy-start.2 = (bf16[64,256]{1,0:T(8,128)(2,1)S(1)}, bf16[64,256]{1,0:T(8,128)(2,1)}, u32[]{:S(2)}) copy-start(bf16[64,256]{1,0:T(8,128)(2,1)} %wo_hbm.1) | copy-start | bytes 98308
  2.7 0.7 copy-start.4
  3.3 0.7 copy-start.5
  4.0 0.7 copy-start.6
  43.5 0.7 copy-start.3
  44.2 0.7 copy-start.7

commit v4 on v3

v4 whole, which is shorter than its diff:
```python
import functools

import jax
import jax.numpy as jnp
from jax import lax
from jax.experimental import pallas as pl
from jax.experimental.pallas import tpu as pltpu
from jax.sharding import PartitionSpec as P

HEAD_DIM = 64
RING = 4
EPS = 1e-06
LOG2E = 1.4426950408889634
F32 = jnp.float32
BF16 = jnp.bfloat16
MESH = pl.DeviceIdType.MESH


def rcopy(src, dst, send, recv, device):
    return pltpu.make_async_remote_copy(
        src_ref=src, dst_ref=dst, send_sem=send, recv_sem=recv, device_id=device, device_id_type=MESH
    )


def places():
    sp, dp = lax.axis_index("sp"), lax.axis_index("dp")
    z, y = lax.div(sp, RING), lax.rem(sp, RING)
    x, c = lax.div(dp, 2), lax.rem(dp, 2)

    def at(dz=0, dy=0, dx=0, dc=0):
        nz, ny = lax.rem(z + dz, RING), lax.rem(y + dy, RING)
        nx, nc = lax.rem(x + dx, RING), lax.rem(c + dc, 2)
        return {"sp": nz * RING + ny, "dp": nx * 2 + nc}

    return z, y, x, c, at


def layer_kernel(
    x_hbm, gain_hbm, wq_hbm, wk_hbm, wv_hbm, wo_hbm, b_hbm, g_hbm,
    ho_ref, wo_ref,
    qv_ref, kk_ref, keys_t, qa, vv, tri, part, rsum, acc, car, stage, h_s, h_r, b_ref, g_all,
    packs, w_all, xg, stage_qv, stage_k,
    wy_s, wy_r, wx_s, wx_r, wf_s, wf_r, wc_s, wc_r, xd_s, xd_r, xf_s, xf_r, a_s, a_r, b_s, b_r,
    oz_s, oz_r, oy_s, oy_r, ox_s, ox_r, of_s, of_r, oc_s, oc_r, local_sem,
    x_ref, gain_ref, wq_ref, wk_ref, wv_ref, wo_in,
):
    z, y, x, c, at = places()
    loads = [
        pltpu.make_async_copy(s, d, local_sem.at[i])
        for i, (s, d) in enumerate(
            (
                (wq_hbm, wq_ref), (wk_hbm, wk_ref), (wv_hbm, wv_ref), (wo_hbm, wo_in),
                (gain_hbm, gain_ref), (x_hbm, x_ref), (b_hbm, b_ref), (g_hbm, g_all),
            )
        )
    ]
    for load in loads:
        load.start()
    friends = [at(dz=i, dy=j) for i in range(RING) for j in range(RING) if i or j]
    friends += [at(dx=1), at(dx=3), at(dc=1)]
    barrier = pltpu.get_barrier_semaphore()
    for f in friends:
        pl.semaphore_signal(barrier, inc=1, device_id=f, device_id_type=MESH)
    for load in loads:
        load.wait()
    rows = x_ref.shape[0]
    half = rows // 2
    depth = wq_ref.shape[1]
    qn, kn = wq_ref.shape[0], wk_ref.shape[0]
    piece_rows = qn + 2 * kn
    packs[c, x, y] = jnp.concatenate([wq_ref[...], wk_ref[...], wv_ref[...]], axis=0)

    def wo_cols(dx, cc):
        return pl.ds(pl.multiple_of((lax.rem(x + dx, RING) * 2 + cc) * depth, depth), depth)

    wo_ref[y, z, :, wo_cols(0, c)] = wo_in[...]
    pl.semaphore_wait(barrier, len(friends))

    sent = []

    def go(copy):
        copy.start()
        sent.append(copy)

    def near(d, axis):
        return at(**{axis: 1 if d == 0 else 3})

    def back(d):
        return 3 if d == 0 else 1

    lo, hi = pl.ds(0, half), pl.ds(half, half)
    halves = (lo, hi)

    def oz(dz, n):
        return wo_ref.at[y, lax.rem(z + dz, RING), n, wo_cols(0, c)]

    every = slice(None)

    def oz_out(dz):
        return rcopy(wo_in, oz(0, every), oz_s.at[dz], oz_r.at[dz], at(dz=dz))

    def oz_in(dz):
        s = oz(RING - dz, every)
        return rcopy(s, s, oz_s.at[dz], oz_r.at[dz], at(dz=dz))

    def x_out(d, i):
        p = halves[i if d == 0 else 1 - i]
        return rcopy(x_ref.at[p], xg.at[d, p], xd_s.at[d, i], xd_r.at[d, i], near(d, "dz"))

    def x_in(d, i):
        p = halves[i if d == 0 else 1 - i]
        return rcopy(xg.at[d, p], xg.at[d, p], xd_s.at[d, i], xd_r.at[d, i], near(d, "dz"))

    cuts = ((0, 64), (64, 32))

    def far_z(d, i, arrived):
        a, n = cuts[i]
        part = pl.ds(a + (0 if d == 0 else half), n)
        return rcopy(xg.at[2 if arrived else d, part], xg.at[2, part], xf_s.at[d, i], xf_r.at[d, i], near(d, "dz"))

    def piece(o):
        return lax.rem(y + RING - o, RING)

    def w_y(o, arrived):
        p = packs.at[c, x, piece(o) if arrived else y]
        return rcopy(p, p, wy_s.at[o], wy_r.at[o], at(dy=o))

    def w_x(o, d, arrived):
        p = packs.at[c, lax.rem(x + back(d), RING) if arrived else x, piece(o)]
        return rcopy(p, p, wx_s.at[d, o], wx_r.at[d, o], near(d, "dx"))

    def w_far(o, d, dx):
        part = packs.at[c, lax.rem(x + dx, RING), piece(o), pl.ds(0 if d == 0 else piece_rows // 2, piece_rows // 2)]
        return rcopy(part, part, wf_s.at[d, o], wf_r.at[d, o], near(d, "dx"))

    def w_c(dx, arrived):
        slab = packs.at[1 - c if arrived else c, lax.rem(x + dx, RING)]
        return rcopy(slab, slab, wc_s.at[dx], wc_r.at[dx], at(dc=1))

    def oy(d, arrived):
        s = wo_ref.at[lax.rem(y + back(d), RING) if arrived else y, :, :, wo_cols(0, c)]
        return rcopy(s, s, oy_s.at[d, 0], oy_r.at[d, 0], near(d, "dy"))

    def oy_far(d, dy):
        s = wo_ref.at[lax.rem(y + dy, RING), pl.ds(0 if d == 0 else 2, 2), :, wo_cols(0, c)]
        return rcopy(s, s, oy_s.at[d, 1], oy_r.at[d, 1], near(d, "dy"))

    def ox(o, d, arrived):
        s = wo_ref.at[piece(o), :, :, wo_cols(back(d) if arrived else 0, c)]
        return rcopy(s, s, ox_s.at[d, o], ox_r.at[d, o], near(d, "dx"))

    def ox_far(o, d, dx):
        s = wo_ref.at[piece(o), pl.ds(0 if d == 0 else 2, 2), :, wo_cols(dx, c)]
        return rcopy(s, s, of_s.at[d, o], of_r.at[d, o], near(d, "dx"))

    def oc(dx, arrived):
        s = wo_ref.at[:, :, :, wo_cols(dx, 1 - c if arrived else c)]
        return rcopy(s, s, oc_s.at[dx], oc_r.at[dx], at(dc=1))

    with jax.named_scope("issue"):
        for o in (1, 3, 2):
            go(w_y(o, False))
        for d in (0, 1):
            go(w_x(0, d, False))
        for dz in (2, 1, 3):
            go(oz_out(dz))
        for i in (0, 1):
            for d in (0, 1):
                go(x_out(d, i))
    with jax.named_scope("wait_wy"):
        for o in (1, 3, 2):
            w_y(o, True).wait_recv()
            for d in (0, 1):
                go(w_x(o, d, False))
        go(w_c(0, False))
    with jax.named_scope("wait_oz"):
        for dz in (1, 3, 2):
            oz_in(dz).wait_recv()
        for d in (0, 1):
            go(oy(d, False))
    with jax.named_scope("wait_wx"):
        for o in (0, 1, 3, 2):
            for d in (0, 1):
                w_x(o, d, True).wait_recv()
                go(w_far(o, d, back(d)))
        go(w_c(3, False))
        go(w_c(1, False))
        for d in (0, 1):
            go(ox(0, d, False))
    with jax.named_scope("wait_oy"):
        for d in (0, 1):
            oy(d, True).wait_recv()
            go(oy_far(d, back(d)))
        for o in (1, 3):
            for d in (0, 1):
                go(ox(o, d, False))
    pending = [[], [], [], []]

    def chunk(n, source, segments, stage_at):
        wide = source.astype(F32)
        normed = (
            wide * lax.rsqrt(jnp.mean(wide * wide, axis=-1, keepdims=True) + EPS) * gain_ref[...]
        ).astype(BF16)
        out = jnp.dot(normed, w_all[...], preferred_element_type=F32).astype(BF16)
        total = out.shape[0]
        v = out[:, 320:384]
        k = out[:, 256:320].reshape(total // 32, 2, 16, HEAD_DIM)
        for i in range(RING):
            stage_qv[i, pl.ds(stage_at, total)] = jnp.concatenate([out[:, i * 64 : i * 64 + 64], v], axis=1)
        stage_k[pl.ds(stage_at // 2, total // 2)] = jnp.concatenate([k[:, 0], k[:, 1]], axis=2).reshape(
            total // 2, 128
        )
        for dz, first, count in segments:
            here, here_k = pl.ds(stage_at, count), pl.ds(stage_at // 2, count // 2)
            nz = lax.rem(z + dz, RING)

            def spot(dy, halved):
                start = (nz * RING + lax.rem(y + dy, RING)) * rows + first
                if halved:
                    return pl.ds(pl.multiple_of(lax.div(start, 2), 16), count // 2)
                return pl.ds(pl.multiple_of(start, 32), count)

            for o in (2, 1, 3):
                ny = lax.rem(y + o, RING)
                go(rcopy(stage_qv.at[ny, here], qv_ref.at[spot(0, False)], a_s.at[n, o], a_r.at[n, o], at(dy=o)))
                go(rcopy(stage_k.at[here_k], kk_ref.at[spot(0, True)], b_s.at[n, o], b_r.at[n, o], at(dy=o)))
            qv_ref[spot(0, False)] = stage_qv[y, here]
            kk_ref[spot(0, True)] = stage_k[here_k]
            for o in (1, 3, 2):
                s, t = qv_ref.at[spot(RING - o, False)], kk_ref.at[spot(RING - o, True)]
                pending[dz].append(rcopy(s, s, a_s.at[n, o], a_r.at[n, o], at(dy=o)))
                pending[dz].append(rcopy(t, t, b_s.at[n, o], b_r.at[n, o], at(dy=o)))
            n, stage_at = n + 1, stage_at + count

    ratio = BLOCK_Q // BLOCK_K
    me = z * RING + y

    def place(dz):
        return lax.rem(z + dz, RING)

    def block_rows(i, size):
        return pl.ds(pl.multiple_of(i * size, size), size)

    def prepare(dz):
        for w in pending[dz]:
            w.wait_recv()
        i = place(dz)
        at_rows = block_rows(i, BLOCK_Q)
        packed = kk_ref[block_rows(i, BLOCK_Q // 2), :].reshape(BLOCK_Q // 32, 16, 128)
        k = jnp.concatenate([packed[:, :, 0:64], packed[:, :, 64:128]], axis=1).reshape(BLOCK_Q, HEAD_DIM)
        kk = k.astype(F32) * (LOG2E / 8.0)
        hi_part = kk.astype(BF16)
        lo_part = (kk - hi_part.astype(F32)).astype(BF16)
        keys_t[0:128, at_rows] = jnp.concatenate([hi_part, lo_part], axis=1).T
        both = qv_ref[at_rows, :]
        qa[at_rows, 0:128] = jnp.concatenate([both[:, 0:64], both[:, 0:64]], axis=1)
        vv[at_rows, :] = both[:, 64:128]

    def block(q, j, carry, diagonal=False):
        count = q.shape[0]
        cols = block_rows(j, BLOCK_K)
        l2 = jnp.dot(q, keys_t[:, cols], preferred_element_type=F32)
        if diagonal:
            t = lax.broadcasted_iota(jnp.int32, (BLOCK_K, BLOCK_K), 0)
            u = lax.broadcasted_iota(jnp.int32, (BLOCK_K, BLOCK_K), 1)
            first = jnp.where(u < t, l2[0:BLOCK_K], -1e30)
            l2 = first if count == BLOCK_K else jnp.concatenate([first, l2[BLOCK_K:]], axis=0)
        soft = jnp.maximum(l2, jnp.log2(1.0 + jnp.exp2(jnp.minimum(l2, 100.0))))
        drop = soft.astype(BF16)
        after = jnp.dot(drop, tri[...], preferred_element_type=F32)
        e = (l2 - soft) - after
        if carry is not None:
            e = e - jnp.concatenate([carry] * (BLOCK_K // 128), axis=1)
        pv = jnp.dot(jnp.exp2(e).astype(BF16), vv[cols, :], preferred_element_type=F32)
        whole = jnp.broadcast_to(after[:, 0:1] + soft[:, 0:1], (count, 128))
        return pv, whole if carry is None else carry + whole

    def diagonal(dz):
        i = place(dz)
        q = qa[block_rows(i, BLOCK_Q), 0:144]
        carry, total = None, None
        for d in reversed(range(ratio)):
            if carry is not None:
                carry = jnp.concatenate([jnp.zeros((BLOCK_K, 128), F32), carry], axis=0)
            pv, carry = block(q[d * BLOCK_K :], i * ratio + d, carry, True)
            if total is None:
                total = pv
            else:
                total = jnp.concatenate([pv[:BLOCK_K], pv[BLOCK_K:] + total], axis=0)
        part[i, i] = total
        rsum[i, i] = carry

    def pair(da, db):
        a, b = place(da), place(db)
        i, j = jnp.maximum(a, b), jnp.minimum(a, b)
        q = qa[block_rows(i, BLOCK_Q), 0:144]
        carry, total = None, None
        for d in reversed(range(ratio)):
            pv, carry = block(q, j * ratio + d, carry)
            total = pv if total is None else total + pv
        part[i, j] = total
        rsum[i, j] = carry

    def finish(i):
        acc[...] = part[i, i]
        car[...] = rsum[i, i]

        def add(n, _):
            j = i - 1 - n
            acc[...] += jnp.exp2(-car[...])[:, 0:HEAD_DIM] * part[i, j]
            car[...] += rsum[i, j]
            return 0

        lax.fori_loop(0, i, add, 0)
        pair_gain = g_all[0:1, block_rows(lax.div(me, 2), 128)]
        own_gain = jnp.where(lax.rem(me, 2) == 0, pair_gain[:, 0:64], pair_gain[:, 64:128])
        a = acc[...]
        scaled = a * lax.rsqrt(jnp.mean(a * a, axis=-1, keepdims=True) + EPS)
        head = (scaled * own_gain).astype(BF16)
        for yy in range(RING):
            mine = head[yy * rows : (yy + 1) * rows]
            stage[i * RING + yy] = jnp.concatenate([mine[:half], mine[half:]], axis=1)
        for yy in range(RING):
            dest = i * RING + yy

            @pl.when(dest != me)
            def _():
                rcopy(
                    stage.at[dest], ho_ref.at[y * RING + z], h_s.at[dest], h_r.at[me],
                    {"sp": dest, "dp": lax.axis_index("dp")},
                ).start()

            @pl.when(dest == me)
            def _():
                ho_ref[y * RING + z] = stage[dest]

    with jax.named_scope("constants"):
        r = lax.broadcasted_iota(jnp.int32, (BLOCK_K, BLOCK_K), 0)
        u = lax.broadcasted_iota(jnp.int32, (BLOCK_K, BLOCK_K), 1)
        tri[...] = jnp.where(r > u, 1.0, 0.0).astype(BF16)
        length = qv_ref.shape[0]
        lane = lax.broadcasted_iota(jnp.int32, (length, 128), 1)
        qa[:, 128:256] = jnp.where(lane < 3, 1.0, 0.0).astype(BF16)
        bb = b_ref[...] * LOG2E
        bh = bb.astype(BF16)
        r1 = bb - bh.astype(F32)
        bm = r1.astype(BF16)
        bl = (r1 - bm.astype(F32)).astype(BF16)
        keys_t[128:144, :] = jnp.concatenate([bh, bm, bl, jnp.zeros((13, length), BF16)], axis=0)
    with jax.named_scope("wait_wfar"):
        for o in (0, 1, 3, 2):
            for d in (0, 1):
                w_far(o, d, 2).wait_recv()
        go(w_c(2, False))
    with jax.named_scope("wait_x0"):
        for d in (0, 1):
            x_in(d, 0).wait_recv()
            for i in (0, 1):
                go(far_z(d, i, False))
    with jax.named_scope("wait_oyfar"):
        for d in (0, 1):
            oy_far(d, 2).wait_recv()
        for d in (0, 1):
            go(ox(2, d, False))
        go(oc(0, False))
    with jax.named_scope("wait_wc"):
        for dx in (0, 3, 1, 2):
            w_c(dx, True).wait_recv()
    with jax.named_scope("assemble"):
        for n in range(2 * RING):
            p = [packs[n % 2, n // 2, i] for i in range(RING)]
            w_all[n * depth : (n + 1) * depth, :] = jnp.concatenate(
                [t[0:qn] for t in p] + [t[qn : qn + kn] for t in p] + [t[qn + kn :] for t in p], axis=0
            ).T
    with jax.named_scope("chunk0"):
        chunk(0, x_ref[...], ((0, 0, rows),), 0)
    with jax.named_scope("chunk12"):
        chunk(1, jnp.concatenate([xg[0, lo], xg[1, hi]], axis=0), ((3, 0, half), (1, half, half)), rows)
    with jax.named_scope("wait_ox"):
        for o in (0, 1, 3):
            for d in (0, 1):
                ox(o, d, True).wait_recv()
                go(ox_far(o, d, back(d)))
    with jax.named_scope("wait_x1"):
        x_in(0, 1).wait_recv()
        x_in(1, 1).wait_recv()
    with jax.named_scope("chunk34"):
        chunk(3, jnp.concatenate([xg[0, hi], xg[1, lo]], axis=0), ((3, half, half), (1, 0, half)), 2 * rows)
    with jax.named_scope("wait_ox2"):
        for d in (0, 1):
            ox(2, d, True).wait_recv()
            go(ox_far(2, d, back(d)))
        go(oc(3, False))
        go(oc(1, False))
    with jax.named_scope("prepare_own"):
        prepare(0)
    with jax.named_scope("diagonal_own"):
        diagonal(0)

    def far_chunk(i):
        a, count = cuts[i]
        with jax.named_scope("wait_far%d" % i):
            for d in (0, 1):
                far_z(d, i, True).wait_recv()
        with jax.named_scope("chunk_far%d" % i):
            chunk(
                5 + 2 * i,
                jnp.concatenate([xg[2, pl.ds(a, count)], xg[2, pl.ds(a + half, count)]], axis=0),
                ((2, a, count), (2, a + half, count)),
                3 * rows + 2 * i * cuts[0][1],
            )

    far_chunk(0)
    far_chunk(1)
    with jax.named_scope("wait_oxfar"):
        for o in (0, 1, 3, 2):
            for d in (0, 1):
                ox_far(o, d, 2).wait_recv()
        go(oc(2, False))
    with jax.named_scope("prepare_near"):
        prepare(3)
        prepare(1)
    with jax.named_scope("diagonal_near"):

        @pl.loop(0, 2)
        def _(n):
            diagonal(3 - 2 * n)

    with jax.named_scope("pairs_near"):

        @pl.loop(0, 3)
        def _(n):
            pair(jnp.where(n == 2, 3, 0), jnp.where(n == 0, 3, 1))

    far = place(2)
    with jax.named_scope("finish_early"):

        @pl.loop(0, far)
        def _(i):
            finish(i)

    with jax.named_scope("prepare_far"):
        prepare(2)
    with jax.named_scope("diagonal_far"):
        diagonal(2)
    with jax.named_scope("pairs_far"):

        @pl.loop(0, 3)
        def _(n):
            pair(2, jnp.where(n == 0, 0, jnp.where(n == 1, 3, 1)))

    with jax.named_scope("finish_late"):

        @pl.loop(far, RING)
        def _(i):
            finish(i)

    with jax.named_scope("wait_ho"):
        for dz in range(RING):
            for dy in range(RING):
                if dz or dy:
                    nz, ny = lax.rem(z + dz, RING), lax.rem(y + dy, RING)
                    other = nz * RING + ny
                    slot = ho_ref.at[ny * RING + nz]
                    w = rcopy(slot, slot, h_s.at[other], h_r.at[other], at(dz=dz, dy=dy))
                    w.wait_recv()
                    w.wait_send()
    with jax.named_scope("wait_oc"):
        for dx in (0, 3, 1, 2):
            oc(dx, True).wait_recv()
    with jax.named_scope("wait_send"):
        for t in sent:
            t.wait_send()


BLOCK_Q = 768
BLOCK_K = 256


def layer(x, gain, wq, wk, wv, wo, bias, out_gain):
    rows, width = x.shape
    length = rows * RING * RING
    depth = wq.shape[1]
    dma = pltpu.SemaphoreType.DMA
    vmem = pl.BlockSpec(memory_space=pltpu.VMEM)
    operands = [
        pltpu.with_memory_space_constraint(t, pltpu.HBM) for t in (x, gain, wq, wk, wv, wo, bias, out_gain)
    ]
    return pl.pallas_call(
        layer_kernel,
        name="layer",
        out_shape=(
            jax.ShapeDtypeStruct((RING * RING, rows // 2, 2 * HEAD_DIM), BF16),
            jax.ShapeDtypeStruct((RING, RING, wo.shape[0], wo.shape[1] * 2 * RING), BF16),
        ),
        in_specs=[pl.BlockSpec(memory_space=pltpu.HBM)] * 8,
        out_specs=(vmem, vmem),
        scratch_shapes=[
            pltpu.VMEM((length, 128), BF16),
            pltpu.VMEM((length // 2, 128), BF16),
            pltpu.VMEM((144, length), BF16),
            pltpu.VMEM((length, 256), BF16),
            pltpu.VMEM((length, HEAD_DIM), BF16),
            pltpu.VMEM((BLOCK_K, BLOCK_K), BF16),
            pltpu.VMEM((RING, RING, BLOCK_Q, HEAD_DIM), F32),
            pltpu.VMEM((RING, RING, BLOCK_Q, 128), F32),
            pltpu.VMEM((BLOCK_Q, HEAD_DIM), F32),
            pltpu.VMEM((BLOCK_Q, 128), F32),
            pltpu.VMEM((RING * RING, rows // 2, 2 * HEAD_DIM), BF16),
            dma((RING * RING,)), dma((RING * RING,)),
            pltpu.VMEM(bias.shape, F32), pltpu.VMEM(out_gain.shape, F32),
            pltpu.VMEM((2, RING, RING, 96, depth), BF16),
            pltpu.VMEM((width, 384), BF16),
            pltpu.VMEM((3, rows, width), BF16),
            pltpu.VMEM((RING, RING * rows, 128), BF16),
            pltpu.VMEM((RING * rows // 2, 128), BF16),
            dma((4,)), dma((4,)), dma((2, 4)), dma((2, 4)), dma((2, 4)), dma((2, 4)), dma((4,)), dma((4,)),
            dma((2, 2)), dma((2, 2)), dma((2, 2)), dma((2, 2)),
            dma((9, 4)), dma((9, 4)), dma((9, 4)), dma((9, 4)),
            dma((4,)), dma((4,)), dma((2, 2)), dma((2, 2)), dma((2, 4)), dma((2, 4)),
            dma((2, 4)), dma((2, 4)), dma((4,)), dma((4,)), dma((8,)),
            pltpu.VMEM(x.shape, BF16), pltpu.VMEM(gain.shape, F32), pltpu.VMEM(wq.shape, BF16),
            pltpu.VMEM(wk.shape, BF16), pltpu.VMEM(wv.shape, BF16), pltpu.VMEM(wo.shape, BF16),
        ],
        compiler_params=pltpu.CompilerParams(
            collective_id=0, has_side_effects=True, vmem_limit_bytes=44 << 20
        ),
    )(*operands)


def mix_kernel(ho_ref, wo_ref, o_ref, lhs):
    heads, half, _ = ho_ref.shape
    for n in range(0, heads, 2):
        a, b = ho_ref[n], ho_ref[n + 1]
        cols = pl.ds(n * HEAD_DIM, 2 * HEAD_DIM)
        lhs[0:half, cols] = jnp.concatenate([a[:, 0:64], b[:, 0:64]], axis=1)
        lhs[half : 2 * half, cols] = jnp.concatenate([a[:, 64:128], b[:, 64:128]], axis=1)
    width = o_ref.shape[1]
    for n in range(0, width, 512):
        o_ref[:, n : n + 512] = jnp.dot(
            lhs[...], wo_ref[:, n : n + 512], preferred_element_type=F32
        ).astype(BF16)


def mix(ho, wo):
    heads, half, _ = ho.shape
    vmem = pl.BlockSpec(memory_space=pltpu.VMEM)
    return pl.pallas_call(
        mix_kernel,
        name="mix",
        out_shape=jax.ShapeDtypeStruct((2 * half, wo.shape[1]), BF16),
        in_specs=[vmem] * 2,
        out_specs=vmem,
        scratch_shapes=[pltpu.VMEM((2 * half, heads * HEAD_DIM), BF16)],
        compiler_params=pltpu.CompilerParams(vmem_limit_bytes=16 << 20),
    )(ho, wo)


def body(inputs, in_gain, w_query, w_key, w_value, key_bias, out_gain, w_out):
    ho, wo = layer(
        inputs[0], in_gain[None], w_query.T, w_key.T, w_value.T, w_out, key_bias[0].T, out_gain[None]
    )
    return mix(ho, wo.reshape(-1, wo.shape[-1]))[None]


def solution(mesh):
    placed = (
        P("dp", "sp", None), P(), P("dp", "sp"), P("dp", "sp"), P("dp", "sp"),
        P("dp", None, "sp"), P(), P("sp", "dp"),
    )
    return jax.shard_map(body, mesh=mesh, in_specs=placed, out_specs=P("dp", "sp", None), check_vma=False)
```

time: 72.4 us -> 60 us (0.83)
  Pallas kernels: 65.8 us -> 59.3 us
  local copies, waits for them, and re-layouts: 6.12 us -> 0 us
    pallas_call x2 -> x1, Pallas kernels: 63.8 us -> 57.3 us  [layer(): pl.pallas_call(layer_kernel, name='layer', out_shape=(jax.ShapeDtypeStruc...]
    unnamed x16 -> x0, local copies, waits for them, and re-layouts: 6.12 us -> none
where the time goes in v4:
time: 60 us; the launch traced here: 59.3 us
  Pallas kernels  59.3 us (99%)
    pallas_call x1, Pallas kernels, layer(): pl.pallas_call(layer_kernel, name='layer', out_shape=(jax.ShapeDtypeStruc...  57.3 us
    pallas_call x1, Pallas kernels, mix(): pl.pallas_call(mix_kernel, name='mix', out_shape=jax.ShapeDtypeStruct((2...  1.93 us

profile of v4, /device:TPU:96, one launch (start us, length us, event | category | flops | bytes accessed | tf_op | source)
XLA Modules:
  0.0 59.3 jit_solution(916747738256208777)
XLA Ops:
  0.0 57.3 %layer.1 = (bf16[16,96,128]{2,1,0:T(8,128)(2,1)S(1)}, bf16[4,4,64,2048]{3,2,1,0:T(8,128)(2,1)S(1)}) custom-call(bf16[192,2048]{1,0:T(8,128)(2,1)} %bitcast.10, f32[1,2048]{1,0:T(1,128)} %bitcast.13, bf16[64,256]{1,0:T(8,128)(2,1)} %bitcast.11, bf16[16,256]{1,0:T(8,128)(2,1)} %bitcast.14, bf16[16,256]{1,0:T(8,128)(2,1)} %bitcast.15, bf16[64,256]{1,0:T(8,128)(2,1)} %wo_hbm.1, ...), custom_call_target="tpu_custom_call" | custom-call | tf_op jit(solution)/shard_map/layer/pallas_call | solution.py:489
  57.3 1.9 %mix.1 = bf16[192,2048]{1,0:T(8,128)(2,1)} custom-call(bf16[16,96,128]{2,1,0:T(8,128)(2,1)S(1)} %get-tuple-element.7.ho_ref, bf16[1024,2048]{1,0:T(8,128)(2,1)S(1)} %bitcast.9), custom_call_target="tpu_custom_call" | custom-call | tf_op jit(solution)/shard_map/mix/pallas_call | solution.py:548

commit v5 on v4

--- a/solution.py
+++ b/solution.py
@@ -40,7 +40,7 @@
     ho_ref, wo_ref,
     qv_ref, kk_ref, keys_t, qa, vv, tri, part, rsum, acc, car, stage, h_s, h_r, b_ref, g_all,
     packs, w_all, xg, stage_qv, stage_k,
-    wy_s, wy_r, wx_s, wx_r, wf_s, wf_r, wc_s, wc_r, xd_s, xd_r, xf_s, xf_r, a_s, a_r, b_s, b_r,
+    wa_s, wa_r, wb_s, wb_r, wc_s, wc_r, xd_s, xd_r, xf_s, xf_r, a_s, a_r, b_s, b_r,
     oz_s, oz_r, oy_s, oy_r, ox_s, ox_r, of_s, of_r, oc_s, oc_r, local_sem,
     x_ref, gain_ref, wq_ref, wk_ref, wv_ref, wo_in,
 ):
@@ -57,7 +57,7 @@
     for load in loads:
         load.start()
     friends = [at(dz=i, dy=j) for i in range(RING) for j in range(RING) if i or j]
-    friends += [at(dx=1), at(dx=3), at(dc=1)]
+    friends += [at(dx=1), at(dx=2), at(dx=3), at(dc=1)]
     barrier = pltpu.get_barrier_semaphore()
     for f in friends:
         pl.semaphore_signal(barrier, inc=1, device_id=f, device_id_type=MESH)
@@ -67,8 +67,10 @@
     half = rows // 2
     depth = wq_ref.shape[1]
     qn, kn = wq_ref.shape[0], wk_ref.shape[0]
-    piece_rows = qn + 2 * kn
-    packs[c, x, y] = jnp.concatenate([wq_ref[...], wk_ref[...], wv_ref[...]], axis=0)
+    split = depth // 2
+    own_piece = jnp.concatenate([wq_ref[...], wk_ref[...], wv_ref[...]], axis=0)
+    packs[c, x, y, 0] = own_piece[:, 0:split]
+    packs[c, x, y, 1] = own_piece[:, split:]
 
     def wo_cols(dx, cc):
         return pl.ds(pl.multiple_of((lax.rem(x + dx, RING) * 2 + cc) * depth, depth), depth)
@@ -88,8 +90,6 @@
     def back(d):
         return 3 if d == 0 else 1
 
-    lo, hi = pl.ds(0, half), pl.ds(half, half)
-    halves = (lo, hi)
 
     def oz(dz, n):
         return wo_ref.at[y, lax.rem(z + dz, RING), n, wo_cols(0, c)]
@@ -103,12 +103,18 @@
         s = oz(RING - dz, every)
         return rcopy(s, s, oz_s.at[dz], oz_r.at[dz], at(dz=dz))
 
+    third = rows // 3
+    parts = (
+        (pl.ds(0, 2 * third), pl.ds(2 * third, third)),
+        (pl.ds(third, 2 * third), pl.ds(0, third)),
+    )
+
     def x_out(d, i):
-        p = halves[i if d == 0 else 1 - i]
+        p = parts[d][i]
         return rcopy(x_ref.at[p], xg.at[d, p], xd_s.at[d, i], xd_r.at[d, i], near(d, "dz"))
 
     def x_in(d, i):
-        p = halves[i if d == 0 else 1 - i]
+        p = parts[d][i]
         return rcopy(xg.at[d, p], xg.at[d, p], xd_s.at[d, i], xd_r.at[d, i], near(d, "dz"))
 
     cuts = ((0, 64), (64, 32))
@@ -121,17 +127,24 @@
     def piece(o):
         return lax.rem(y + RING - o, RING)
 
-    def w_y(o, arrived):
-        p = packs.at[c, x, piece(o) if arrived else y]
-        return rcopy(p, p, wy_s.at[o], wy_r.at[o], at(dy=o))
-
-    def w_x(o, d, arrived):
-        p = packs.at[c, lax.rem(x + back(d), RING) if arrived else x, piece(o)]
-        return rcopy(p, p, wx_s.at[d, o], wx_r.at[d, o], near(d, "dx"))
-
-    def w_far(o, d, dx):
-        part = packs.at[c, lax.rem(x + dx, RING), piece(o), pl.ds(0 if d == 0 else piece_rows // 2, piece_rows // 2)]
-        return rcopy(part, part, wf_s.at[d, o], wf_r.at[d, o], near(d, "dx"))
+    def w_first(side, o, arrived):
+        py = piece(o) if arrived and side == 0 else y
+        px = lax.rem(x + RING - o, RING) if arrived and side == 1 else x
+        p = packs.at[c, px, py, side]
+        return rcopy(p, p, wa_s.at[side, o], wa_r.at[side, o], at(dy=o) if side == 0 else at(dx=o))
+
+    def w_second(side, came, o, arrived):
+        py, px = y, x
+        if side == 0:
+            py = piece(came)
+            px = lax.rem(x + RING - o, RING) if arrived else x
+        else:
+            px = lax.rem(x + RING - came, RING)
+            py = piece(o) if arrived else y
+        p = packs.at[c, px, py, side]
+        return rcopy(
+            p, p, wb_s.at[side, came, o], wb_r.at[side, came, o], at(dx=o) if side == 0 else at(dy=o)
+        )
 
     def w_c(dx, arrived):
         slab = packs.at[1 - c if arrived else c, lax.rem(x + dx, RING)]
@@ -158,42 +171,40 @@
         return rcopy(s, s, oc_s.at[dx], oc_r.at[dx], at(dc=1))
 
     with jax.named_scope("issue"):
-        for o in (1, 3, 2):
-            go(w_y(o, False))
-        for d in (0, 1):
-            go(w_x(0, d, False))
+        for o in (2, 1, 3):
+            for side in (0, 1):
+                go(w_first(side, o, False))
+        for o in (2, 1, 3):
+            for side in (0, 1):
+                go(w_second(side, 0, o, False))
         for dz in (2, 1, 3):
             go(oz_out(dz))
         for i in (0, 1):
             for d in (0, 1):
                 go(x_out(d, i))
-    with jax.named_scope("wait_wy"):
-        for o in (1, 3, 2):
-            w_y(o, True).wait_recv()
-            for d in (0, 1):
-                go(w_x(o, d, False))
-        go(w_c(0, False))
+    with jax.named_scope("wait_wfirst"):
+        for came in (1, 3, 2):
+            for side in (0, 1):
+                w_first(side, came, True).wait_recv()
+                for o in (2, 1, 3):
+                    go(w_second(side, came, o, False))
     with jax.named_scope("wait_oz"):
         for dz in (1, 3, 2):
             oz_in(dz).wait_recv()
         for d in (0, 1):
             go(oy(d, False))
-    with jax.named_scope("wait_wx"):
-        for o in (0, 1, 3, 2):
-            for d in (0, 1):
-                w_x(o, d, True).wait_recv()
-                go(w_far(o, d, back(d)))
-        go(w_c(3, False))
-        go(w_c(1, False))
+    with jax.named_scope("wait_wsecond"):
         for d in (0, 1):
             go(ox(0, d, False))
-    with jax.named_scope("wait_oy"):
-        for d in (0, 1):
-            oy(d, True).wait_recv()
-            go(oy_far(d, back(d)))
-        for o in (1, 3):
-            for d in (0, 1):
-                go(ox(o, d, False))
+        for o in (1, 3, 2):
+            w_second(1, 0, o, True).wait_recv()
+        go(w_c(0, False))
+        for px in (1, 3, 2):
+            for came in (0, 1, 3, 2):
+                w_second(0, came, px, True).wait_recv()
+            for o in (1, 3, 2):
+                w_second(1, px, o, True).wait_recv()
+            go(w_c(RING - px, False))
     pending = [[], [], [], []]
 
     def chunk(n, source, segments, stage_at):
@@ -347,56 +358,58 @@
         bm = r1.astype(BF16)
         bl = (r1 - bm.astype(F32)).astype(BF16)
         keys_t[128:144, :] = jnp.concatenate([bh, bm, bl, jnp.zeros((13, length), BF16)], axis=0)
-    with jax.named_scope("wait_wfar"):
-        for o in (0, 1, 3, 2):
-            for d in (0, 1):
-                w_far(o, d, 2).wait_recv()
-        go(w_c(2, False))
-    with jax.named_scope("wait_x0"):
-        for d in (0, 1):
-            x_in(d, 0).wait_recv()
-            for i in (0, 1):
-                go(far_z(d, i, False))
-    with jax.named_scope("wait_oyfar"):
-        for d in (0, 1):
-            oy_far(d, 2).wait_recv()
-        for d in (0, 1):
-            go(ox(2, d, False))
-        go(oc(0, False))
     with jax.named_scope("wait_wc"):
         for dx in (0, 3, 1, 2):
             w_c(dx, True).wait_recv()
     with jax.named_scope("assemble"):
         for n in range(2 * RING):
-            p = [packs[n % 2, n // 2, i] for i in range(RING)]
-            w_all[n * depth : (n + 1) * depth, :] = jnp.concatenate(
-                [t[0:qn] for t in p] + [t[qn : qn + kn] for t in p] + [t[qn + kn :] for t in p], axis=0
-            ).T
+            for side in (0, 1):
+                p = [packs[n % 2, n // 2, i, side] for i in range(RING)]
+                first = n * depth + side * split
+                w_all[first : first + split, :] = jnp.concatenate(
+                    [t[0:qn] for t in p] + [t[qn : qn + kn] for t in p] + [t[qn + kn :] for t in p], axis=0
+                ).T
     with jax.named_scope("chunk0"):
         chunk(0, x_ref[...], ((0, 0, rows),), 0)
+    with jax.named_scope("wait_oy"):
+        for d in (0, 1):
+            oy(d, True).wait_recv()
+            go(oy_far(d, back(d)))
+        for o in (1, 3):
+            for d in (0, 1):
+                go(ox(o, d, False))
+    with jax.named_scope("wait_x0"):
+        for d in (0, 1):
+            x_in(d, 0).wait_recv()
+            for i in (0, 1):
+                go(far_z(d, i, False))
     with jax.named_scope("chunk12"):
-        chunk(1, jnp.concatenate([xg[0, lo], xg[1, hi]], axis=0), ((3, 0, half), (1, half, half)), rows)
-    with jax.named_scope("wait_ox"):
-        for o in (0, 1, 3):
-            for d in (0, 1):
-                ox(o, d, True).wait_recv()
-                go(ox_far(o, d, back(d)))
+        chunk(
+            1,
+            jnp.concatenate([xg[0, parts[0][0]], xg[1, parts[1][0]]], axis=0),
+            ((3, 0, 2 * third), (1, third, 2 * third)),
+            rows,
+        )
+    with jax.named_scope("prepare_own"):
+        prepare(0)
+    with jax.named_scope("diagonal_own"):
+        diagonal(0)
     with jax.named_scope("wait_x1"):
         x_in(0, 1).wait_recv()
         x_in(1, 1).wait_recv()
     with jax.named_scope("chunk34"):
-        chunk(3, jnp.concatenate([xg[0, hi], xg[1, lo]], axis=0), ((3, half, half), (1, 0, half)), 2 * rows)
-    with jax.named_scope("wait_ox2"):
-        for d in (0, 1):
-            ox(2, d, True).wait_recv()
-            go(ox_far(2, d, back(d)))
-        go(oc(3, False))
-        go(oc(1, False))
-    with jax.named_scope("prepare_own"):
-        prepare(0)
-    with jax.named_scope("diagonal_own"):
-        diagonal(0)
-
+        chunk(
+            3,
+            jnp.concatenate([xg[0, parts[0][1]], xg[1, parts[1][1]]], axis=0),
+            ((3, 2 * third, third), (1, 0, third)),
+            rows + 4 * third,
+        )
+    with jax.named_scope("wait_oyfar"):
+        for d in (0, 1):
+            oy_far(d, 2).wait_recv()
+        for d in (0, 1):
+            go(ox(2, d, False))
+        go(oc(0, False))
     def far_chunk(i):
         a, count = cuts[i]
         with jax.named_scope("wait_far%d" % i):
@@ -410,29 +423,36 @@
                 3 * rows + 2 * i * cuts[0][1],
             )
 
+    with jax.named_scope("wait_ox"):
+        for o in (0, 1, 3):
+            for d in (0, 1):
+                ox(o, d, True).wait_recv()
+                go(ox_far(o, d, back(d)))
+
+    with jax.named_scope("prepare_near"):
+        prepare(3)
+        prepare(1)
     far_chunk(0)
     far_chunk(1)
+    with jax.named_scope("wait_ox2"):
+        for d in (0, 1):
+            ox(2, d, True).wait_recv()
+            go(ox_far(2, d, back(d)))
+        go(oc(3, False))
+        go(oc(1, False))
+    with jax.named_scope("blocks_near"):
+        diagonal(3)
+        diagonal(1)
+        pair(0, 3)
+        pair(0, 1)
+        pair(3, 1)
+
+    far = place(2)
     with jax.named_scope("wait_oxfar"):
         for o in (0, 1, 3, 2):
             for d in (0, 1):
                 ox_far(o, d, 2).wait_recv()
         go(oc(2, False))
-    with jax.named_scope("prepare_near"):
-        prepare(3)
-        prepare(1)
-    with jax.named_scope("diagonal_near"):
-
-        @pl.loop(0, 2)
-        def _(n):
-            diagonal(3 - 2 * n)
-
-    with jax.named_scope("pairs_near"):
-
-        @pl.loop(0, 3)
-        def _(n):
-            pair(jnp.where(n == 2, 3, 0), jnp.where(n == 0, 3, 1))
-
-    far = place(2)
     with jax.named_scope("finish_early"):
 
         @pl.loop(0, far)
@@ -441,14 +461,11 @@
 
     with jax.named_scope("prepare_far"):
         prepare(2)
-    with jax.named_scope("diagonal_far"):
+    with jax.named_scope("blocks_far"):
         diagonal(2)
-    with jax.named_scope("pairs_far"):
-
-        @pl.loop(0, 3)
-        def _(n):
-            pair(2, jnp.where(n == 0, 0, jnp.where(n == 1, 3, 1)))
-
+        pair(2, 0)
+        pair(2, 3)
+        pair(2, 1)
     with jax.named_scope("finish_late"):
 
         @pl.loop(far, RING)
@@ -509,12 +526,12 @@
             pltpu.VMEM((RING * RING, rows // 2, 2 * HEAD_DIM), BF16),
             dma((RING * RING,)), dma((RING * RING,)),
             pltpu.VMEM(bias.shape, F32), pltpu.VMEM(out_gain.shape, F32),
-            pltpu.VMEM((2, RING, RING, 96, depth), BF16),
+            pltpu.VMEM((2, RING, RING, 2, 96, depth // 2), BF16),
             pltpu.VMEM((width, 384), BF16),
             pltpu.VMEM((3, rows, width), BF16),
             pltpu.VMEM((RING, RING * rows, 128), BF16),
             pltpu.VMEM((RING * rows // 2, 128), BF16),
-            dma((4,)), dma((4,)), dma((2, 4)), dma((2, 4)), dma((2, 4)), dma((2, 4)), dma((4,)), dma((4,)),
+            dma((2, 4)), dma((2, 4)), dma((2, 4, 4)), dma((2, 4, 4)), dma((4,)), dma((4,)),
             dma((2, 2)), dma((2, 2)), dma((2, 2)), dma((2, 2)),
             dma((9, 4)), dma((9, 4)), dma((9, 4)), dma((9, 4)),
             dma((4,)), dma((4,)), dma((2, 2)), dma((2, 2)), dma((2, 4)), dma((2, 4)),

time: 60 us -> 57.7 us (0.962)
  Pallas kernels: 59.3 us -> 56.6 us
    pallas_call x1, Pallas kernels: 57.3 us -> 54.7 us  [layer(): pl.pallas_call(layer_kernel, name='layer', out_shape=(jax.ShapeDtypeStruc...]
where the time goes in v5:
time: 57.7 us; the launch traced here: 56.6 us
  Pallas kernels  56.6 us (98%)
    pallas_call x1, Pallas kernels, layer(): pl.pallas_call(layer_kernel, name='layer', out_shape=(jax.ShapeDtypeStruc...  54.7 us
    pallas_call x1, Pallas kernels, mix(): pl.pallas_call(mix_kernel, name='mix', out_shape=jax.ShapeDtypeStruct((2...  1.93 us

profile of v5, /device:TPU:96, one launch (start us, length us, event | category | flops | bytes accessed | tf_op | source)
XLA Modules:
  0.0 56.6 jit_solution(16650419947254771409)
XLA Ops:
  0.0 54.7 %layer.1 = (bf16[16,96,128]{2,1,0:T(8,128)(2,1)S(1)}, bf16[4,4,64,2048]{3,2,1,0:T(8,128)(2,1)S(1)}) custom-call(bf16[192,2048]{1,0:T(8,128)(2,1)} %bitcast.10, f32[1,2048]{1,0:T(1,128)} %bitcast.13, bf16[64,256]{1,0:T(8,128)(2,1)} %bitcast.11, bf16[16,256]{1,0:T(8,128)(2,1)} %bitcast.14, bf16[16,256]{1,0:T(8,128)(2,1)} %bitcast.15, bf16[64,256]{1,0:T(8,128)(2,1)} %wo_hbm.1, ...), custom_call_target="tpu_custom_call" | custom-call | tf_op jit(solution)/shard_map/layer/pallas_call | solution.py:506
  54.7 1.9 %mix.1 = bf16[192,2048]{1,0:T(8,128)(2,1)} custom-call(bf16[16,96,128]{2,1,0:T(8,128)(2,1)S(1)} %get-tuple-element.7.ho_ref, bf16[1024,2048]{1,0:T(8,128)(2,1)S(1)} %bitcast.9), custom_call_target="tpu_custom_call" | custom-call | tf_op jit(solution)/shard_map/mix/pallas_call | solution.py:565

commit v6 on v5

--- a/solution.py
+++ b/solution.py
@@ -40,7 +40,7 @@
     ho_ref, wo_ref,
     qv_ref, kk_ref, keys_t, qa, vv, tri, part, rsum, acc, car, stage, h_s, h_r, b_ref, g_all,
     packs, w_all, xg, stage_qv, stage_k,
-    wa_s, wa_r, wb_s, wb_r, wc_s, wc_r, xd_s, xd_r, xf_s, xf_r, a_s, a_r, b_s, b_r,
+    wa_s, wa_r, wb_s, wb_r, wc_s, wc_r, xd_s, xd_r, xf_s, xf_r, a_s, a_r,
     oz_s, oz_r, oy_s, oy_r, ox_s, ox_r, of_s, of_r, oc_s, oc_r, local_sem,
     x_ref, gain_ref, wq_ref, wk_ref, wv_ref, wo_in,
 ):
@@ -68,6 +68,7 @@
     depth = wq_ref.shape[1]
     qn, kn = wq_ref.shape[0], wk_ref.shape[0]
     split = depth // 2
+    piece_rows = qn + 2 * kn
     own_piece = jnp.concatenate([wq_ref[...], wk_ref[...], wv_ref[...]], axis=0)
     packs[c, x, y, 0] = own_piece[:, 0:split]
     packs[c, x, y, 1] = own_piece[:, split:]
@@ -78,11 +79,12 @@
     wo_ref[y, z, :, wo_cols(0, c)] = wo_in[...]
     pl.semaphore_wait(barrier, len(friends))
 
-    sent = []
-
     def go(copy):
         copy.start()
-        sent.append(copy)
+
+    def settle(sem, count):
+        ref = qv_ref.at[pl.ds(0, count)]
+        pltpu.make_async_copy(ref, ref, sem).wait()
 
     def near(d, axis):
         return at(**{axis: 1 if d == 0 else 3})
@@ -95,13 +97,10 @@
         return wo_ref.at[y, lax.rem(z + dz, RING), n, wo_cols(0, c)]
 
     every = slice(None)
+    wo_rows = wo_in.shape[0] * wo_in.shape[1] // 128
 
     def oz_out(dz):
-        return rcopy(wo_in, oz(0, every), oz_s.at[dz], oz_r.at[dz], at(dz=dz))
-
-    def oz_in(dz):
-        s = oz(RING - dz, every)
-        return rcopy(s, s, oz_s.at[dz], oz_r.at[dz], at(dz=dz))
+        return rcopy(wo_in, oz(0, every), oz_s, oz_r, at(dz=dz))
 
     third = rows // 3
     parts = (
@@ -111,18 +110,18 @@
 
     def x_out(d, i):
         p = parts[d][i]
-        return rcopy(x_ref.at[p], xg.at[d, p], xd_s.at[d, i], xd_r.at[d, i], near(d, "dz"))
+        return rcopy(x_ref.at[p], xg.at[d, p], xd_s, xd_r.at[d, i], near(d, "dz"))
 
     def x_in(d, i):
         p = parts[d][i]
-        return rcopy(xg.at[d, p], xg.at[d, p], xd_s.at[d, i], xd_r.at[d, i], near(d, "dz"))
+        return rcopy(xg.at[d, p], xg.at[d, p], xd_s, xd_r.at[d, i], near(d, "dz"))
 
     cuts = ((0, 64), (64, 32))
 
-    def far_z(d, i, arrived):
+    def far_z(d, i):
         a, n = cuts[i]
         part = pl.ds(a + (0 if d == 0 else half), n)
-        return rcopy(xg.at[2 if arrived else d, part], xg.at[2, part], xf_s.at[d, i], xf_r.at[d, i], near(d, "dz"))
+        return rcopy(xg.at[d, part], xg.at[2, part], xf_s, xf_r.at[i], near(d, "dz"))
 
     def piece(o):
         return lax.rem(y + RING - o, RING)
@@ -131,44 +130,35 @@
         py = piece(o) if arrived and side == 0 else y
         px = lax.rem(x + RING - o, RING) if arrived and side == 1 else x
         p = packs.at[c, px, py, side]
-        return rcopy(p, p, wa_s.at[side, o], wa_r.at[side, o], at(dy=o) if side == 0 else at(dx=o))
-
-    def w_second(side, came, o, arrived):
-        py, px = y, x
-        if side == 0:
-            py = piece(came)
-            px = lax.rem(x + RING - o, RING) if arrived else x
-        else:
-            px = lax.rem(x + RING - came, RING)
-            py = piece(o) if arrived else y
-        p = packs.at[c, px, py, side]
-        return rcopy(
-            p, p, wb_s.at[side, came, o], wb_r.at[side, came, o], at(dx=o) if side == 0 else at(dy=o)
-        )
-
-    def w_c(dx, arrived):
-        slab = packs.at[1 - c if arrived else c, lax.rem(x + dx, RING)]
-        return rcopy(slab, slab, wc_s.at[dx], wc_r.at[dx], at(dc=1))
+        return rcopy(p, p, wa_s, wa_r.at[side, o - 1], at(dy=o) if side == 0 else at(dx=o))
+
+    def w_second(side, came, o):
+        p = packs.at[c, lax.rem(x + RING - (came if side else 0), RING), piece(0 if side else came), side]
+        return rcopy(p, p, wb_s, wb_r.at[came if side else o], at(dy=o) if side else at(dx=o))
+
+    def w_c(dx):
+        slab = packs.at[c, lax.rem(x + dx, RING)]
+        return rcopy(slab, slab, wc_s, wc_r, at(dc=1))
 
     def oy(d, arrived):
         s = wo_ref.at[lax.rem(y + back(d), RING) if arrived else y, :, :, wo_cols(0, c)]
-        return rcopy(s, s, oy_s.at[d, 0], oy_r.at[d, 0], near(d, "dy"))
+        return rcopy(s, s, oy_s, oy_r.at[d], near(d, "dy"))
 
     def oy_far(d, dy):
         s = wo_ref.at[lax.rem(y + dy, RING), pl.ds(0 if d == 0 else 2, 2), :, wo_cols(0, c)]
-        return rcopy(s, s, oy_s.at[d, 1], oy_r.at[d, 1], near(d, "dy"))
-
-    def ox(o, d, arrived):
-        s = wo_ref.at[piece(o), :, :, wo_cols(back(d) if arrived else 0, c)]
-        return rcopy(s, s, ox_s.at[d, o], ox_r.at[d, o], near(d, "dx"))
+        return rcopy(s, s, oy_s, oy_r.at[2], near(d, "dy"))
+
+    def ox(o, d):
+        s = wo_ref.at[piece(o), :, :, wo_cols(0, c)]
+        return rcopy(s, s, ox_s, ox_r.at[1 if o == 2 else 0], near(d, "dx"))
 
     def ox_far(o, d, dx):
         s = wo_ref.at[piece(o), pl.ds(0 if d == 0 else 2, 2), :, wo_cols(dx, c)]
-        return rcopy(s, s, of_s.at[d, o], of_r.at[d, o], near(d, "dx"))
-
-    def oc(dx, arrived):
-        s = wo_ref.at[:, :, :, wo_cols(dx, 1 - c if arrived else c)]
-        return rcopy(s, s, oc_s.at[dx], oc_r.at[dx], at(dc=1))
+        return rcopy(s, s, of_s, of_r, near(d, "dx"))
+
+    def oc(dx):
+        s = wo_ref.at[:, :, :, wo_cols(dx, c)]
+        return rcopy(s, s, oc_s, oc_r, at(dc=1))
 
     with jax.named_scope("issue"):
         for o in (2, 1, 3):
@@ -176,7 +166,7 @@
                 go(w_first(side, o, False))
         for o in (2, 1, 3):
             for side in (0, 1):
-                go(w_second(side, 0, o, False))
+                go(w_second(side, 0, o))
         for dz in (2, 1, 3):
             go(oz_out(dz))
         for i in (0, 1):
@@ -187,27 +177,20 @@
             for side in (0, 1):
                 w_first(side, came, True).wait_recv()
                 for o in (2, 1, 3):
-                    go(w_second(side, came, o, False))
+                    go(w_second(side, came, o))
     with jax.named_scope("wait_oz"):
-        for dz in (1, 3, 2):
-            oz_in(dz).wait_recv()
+        settle(oz_r, 3 * wo_rows)
         for d in (0, 1):
             go(oy(d, False))
     with jax.named_scope("wait_wsecond"):
         for d in (0, 1):
-            go(ox(0, d, False))
-        for o in (1, 3, 2):
-            w_second(1, 0, o, True).wait_recv()
-        go(w_c(0, False))
+            go(ox(0, d))
+        settle(wb_r.at[0], 3 * piece_rows)
+        go(w_c(0))
         for px in (1, 3, 2):
-            for came in (0, 1, 3, 2):
-                w_second(0, came, px, True).wait_recv()
-            for o in (1, 3, 2):
-                w_second(1, px, o, True).wait_recv()
-            go(w_c(RING - px, False))
-    pending = [[], [], [], []]
-
-    def chunk(n, source, segments, stage_at):
+            settle(wb_r.at[px], 7 * piece_rows)
+            go(w_c(RING - px))
+    def chunk(source, segments, stage_at):
         wide = source.astype(F32)
         normed = (
             wide * lax.rsqrt(jnp.mean(wide * wide, axis=-1, keepdims=True) + EPS) * gain_ref[...]
@@ -225,23 +208,19 @@
             here, here_k = pl.ds(stage_at, count), pl.ds(stage_at // 2, count // 2)
             nz = lax.rem(z + dz, RING)
 
-            def spot(dy, halved):
-                start = (nz * RING + lax.rem(y + dy, RING)) * rows + first
+            def spot(halved):
+                start = (nz * RING + y) * rows + first
                 if halved:
                     return pl.ds(pl.multiple_of(lax.div(start, 2), 16), count // 2)
                 return pl.ds(pl.multiple_of(start, 32), count)
 
             for o in (2, 1, 3):
                 ny = lax.rem(y + o, RING)
-                go(rcopy(stage_qv.at[ny, here], qv_ref.at[spot(0, False)], a_s.at[n, o], a_r.at[n, o], at(dy=o)))
-                go(rcopy(stage_k.at[here_k], kk_ref.at[spot(0, True)], b_s.at[n, o], b_r.at[n, o], at(dy=o)))
-            qv_ref[spot(0, False)] = stage_qv[y, here]
-            kk_ref[spot(0, True)] = stage_k[here_k]
-            for o in (1, 3, 2):
-                s, t = qv_ref.at[spot(RING - o, False)], kk_ref.at[spot(RING - o, True)]
-                pending[dz].append(rcopy(s, s, a_s.at[n, o], a_r.at[n, o], at(dy=o)))
-                pending[dz].append(rcopy(t, t, b_s.at[n, o], b_r.at[n, o], at(dy=o)))
-            n, stage_at = n + 1, stage_at + count
+                go(rcopy(stage_qv.at[ny, here], qv_ref.at[spot(False)], a_s.at[dz], a_r.at[dz, o - 1], at(dy=o)))
+                go(rcopy(stage_k.at[here_k], kk_ref.at[spot(True)], a_s.at[dz], a_r.at[dz, o - 1], at(dy=o)))
+            qv_ref[spot(False)] = stage_qv[y, here]
+            kk_ref[spot(True)] = stage_k[here_k]
+            stage_at = stage_at + count
 
     ratio = BLOCK_Q // BLOCK_K
     me = z * RING + y
@@ -253,8 +232,8 @@
         return pl.ds(pl.multiple_of(i * size, size), size)
 
     def prepare(dz):
-        for w in pending[dz]:
-            w.wait_recv()
+        for o in range(RING - 1):
+            settle(a_r.at[dz, o], rows + half)
         i = place(dz)
         at_rows = block_rows(i, BLOCK_Q)
         packed = kk_ref[block_rows(i, BLOCK_Q // 2), :].reshape(BLOCK_Q // 32, 16, 128)
@@ -337,7 +316,7 @@
             @pl.when(dest != me)
             def _():
                 rcopy(
-                    stage.at[dest], ho_ref.at[y * RING + z], h_s.at[dest], h_r.at[me],
+                    stage.at[dest], ho_ref.at[y * RING + z], h_s, h_r,
                     {"sp": dest, "dp": lax.axis_index("dp")},
                 ).start()
 
@@ -359,8 +338,7 @@
         bl = (r1 - bm.astype(F32)).astype(BF16)
         keys_t[128:144, :] = jnp.concatenate([bh, bm, bl, jnp.zeros((13, length), BF16)], axis=0)
     with jax.named_scope("wait_wc"):
-        for dx in (0, 3, 1, 2):
-            w_c(dx, True).wait_recv()
+        settle(wc_r, RING * RING * 2 * piece_rows)
     with jax.named_scope("assemble"):
         for n in range(2 * RING):
             for side in (0, 1):
@@ -370,22 +348,21 @@
                     [t[0:qn] for t in p] + [t[qn : qn + kn] for t in p] + [t[qn + kn :] for t in p], axis=0
                 ).T
     with jax.named_scope("chunk0"):
-        chunk(0, x_ref[...], ((0, 0, rows),), 0)
+        chunk(x_ref[...], ((0, 0, rows),), 0)
     with jax.named_scope("wait_oy"):
         for d in (0, 1):
             oy(d, True).wait_recv()
             go(oy_far(d, back(d)))
         for o in (1, 3):
             for d in (0, 1):
-                go(ox(o, d, False))
+                go(ox(o, d))
     with jax.named_scope("wait_x0"):
         for d in (0, 1):
             x_in(d, 0).wait_recv()
             for i in (0, 1):
-                go(far_z(d, i, False))
+                go(far_z(d, i))
     with jax.named_scope("chunk12"):
         chunk(
-            1,
             jnp.concatenate([xg[0, parts[0][0]], xg[1, parts[1][0]]], axis=0),
             ((3, 0, 2 * third), (1, third, 2 * third)),
             rows,
@@ -399,34 +376,30 @@
         x_in(1, 1).wait_recv()
     with jax.named_scope("chunk34"):
         chunk(
-            3,
             jnp.concatenate([xg[0, parts[0][1]], xg[1, parts[1][1]]], axis=0),
             ((3, 2 * third, third), (1, 0, third)),
             rows + 4 * third,
         )
     with jax.named_scope("wait_oyfar"):
+        settle(oy_r.at[2], RING * wo_rows)
         for d in (0, 1):
-            oy_far(d, 2).wait_recv()
-        for d in (0, 1):
-            go(ox(2, d, False))
-        go(oc(0, False))
+            go(ox(2, d))
+        go(oc(0))
     def far_chunk(i):
         a, count = cuts[i]
         with jax.named_scope("wait_far%d" % i):
-            for d in (0, 1):
-                far_z(d, i, True).wait_recv()
+            settle(xf_r.at[i], 2 * count * x_ref.shape[1] // 128)
         with jax.named_scope("chunk_far%d" % i):
             chunk(
-                5 + 2 * i,
                 jnp.concatenate([xg[2, pl.ds(a, count)], xg[2, pl.ds(a + half, count)]], axis=0),
                 ((2, a, count), (2, a + half, count)),
                 3 * rows + 2 * i * cuts[0][1],
             )
 
     with jax.named_scope("wait_ox"):
+        settle(ox_r.at[0], 6 * RING * wo_rows)
         for o in (0, 1, 3):
             for d in (0, 1):
-                ox(o, d, True).wait_recv()
                 go(ox_far(o, d, back(d)))
 
     with jax.named_scope("prepare_near"):
@@ -435,11 +408,11 @@
     far_chunk(0)
     far_chunk(1)
     with jax.named_scope("wait_ox2"):
+        settle(ox_r.at[1], 2 * RING * wo_rows)
         for d in (0, 1):
-            ox(2, d, True).wait_recv()
             go(ox_far(2, d, back(d)))
-        go(oc(3, False))
-        go(oc(1, False))
+        go(oc(3))
+        go(oc(1))
     with jax.named_scope("blocks_near"):
         diagonal(3)
         diagonal(1)
@@ -449,10 +422,8 @@
 
     far = place(2)
     with jax.named_scope("wait_oxfar"):
-        for o in (0, 1, 3, 2):
-            for d in (0, 1):
-                ox_far(o, d, 2).wait_recv()
-        go(oc(2, False))
+        settle(of_r, RING * RING * wo_rows)
+        go(oc(2))
     with jax.named_scope("finish_early"):
 
         @pl.loop(0, far)
@@ -461,33 +432,48 @@
 
     with jax.named_scope("prepare_far"):
         prepare(2)
+    with jax.named_scope("diagonal_far"):
+        diagonal(2)
     with jax.named_scope("blocks_far"):
-        diagonal(2)
-        pair(2, 0)
-        pair(2, 3)
-        pair(2, 1)
-    with jax.named_scope("finish_late"):
-
-        @pl.loop(far, RING)
+
+        @pl.loop(0, RING)
         def _(i):
-            finish(i)
-
+            @pl.when(i < far)
+            def _():
+                pair(2, i - z + RING)
+
+            @pl.when(i > far)
+            def _():
+                pair(2, i - z + RING)
+                finish(i)
+
+            @pl.when(i == far)
+            def _():
+                finish(i)
+
+    whole_w = wo_ref.at[:, :, :, pl.ds(0, RING * depth)]
+    ho_rows = (RING * RING - 1) * half
     with jax.named_scope("wait_ho"):
+        settle(h_r, ho_rows)
+    with jax.named_scope("wait_oc"):
+        pltpu.make_async_copy(whole_w, whole_w, oc_r).wait()
+    with jax.named_scope("wait_send"):
+        settle(h_s, ho_rows)
+        pltpu.make_async_copy(whole_w, whole_w, oc_s).wait()
+        both_x = xg.at[pl.ds(0, 2)]
+        pltpu.make_async_copy(both_x, both_x, xd_s).wait()
+        one_x = xg.at[0]
+        pltpu.make_async_copy(one_x, one_x, xf_s).wait()
+        settle(wa_s, 6 * piece_rows)
+        settle(wb_s, 24 * piece_rows)
+        settle(wc_s, RING * RING * 2 * piece_rows)
+        settle(oz_s, 3 * wo_rows)
+        settle(oy_s, 3 * RING * wo_rows)
+        x_w = wo_ref.at[:, :, :, pl.ds(0, 2 * depth)]
+        pltpu.make_async_copy(x_w, x_w, ox_s).wait()
+        settle(of_s, RING * RING * wo_rows)
         for dz in range(RING):
-            for dy in range(RING):
-                if dz or dy:
-                    nz, ny = lax.rem(z + dz, RING), lax.rem(y + dy, RING)
-                    other = nz * RING + ny
-                    slot = ho_ref.at[ny * RING + nz]
-                    w = rcopy(slot, slot, h_s.at[other], h_r.at[other], at(dz=dz, dy=dy))
-                    w.wait_recv()
-                    w.wait_send()
-    with jax.named_scope("wait_oc"):
-        for dx in (0, 3, 1, 2):
-            oc(dx, True).wait_recv()
-    with jax.named_scope("wait_send"):
-        for t in sent:
-            t.wait_send()
+            settle(a_s.at[dz], 3 * (rows + half))
 
 
 BLOCK_Q = 768
@@ -524,18 +510,18 @@
             pltpu.VMEM((BLOCK_Q, HEAD_DIM), F32),
             pltpu.VMEM((BLOCK_Q, 128), F32),
             pltpu.VMEM((RING * RING, rows // 2, 2 * HEAD_DIM), BF16),
-            dma((RING * RING,)), dma((RING * RING,)),
+            dma(()), dma(()),
             pltpu.VMEM(bias.shape, F32), pltpu.VMEM(out_gain.shape, F32),
             pltpu.VMEM((2, RING, RING, 2, 96, depth // 2), BF16),
             pltpu.VMEM((width, 384), BF16),
             pltpu.VMEM((3, rows, width), BF16),
             pltpu.VMEM((RING, RING * rows, 128), BF16),
             pltpu.VMEM((RING * rows // 2, 128), BF16),
-            dma((2, 4)), dma((2, 4)), dma((2, 4, 4)), dma((2, 4, 4)), dma((4,)), dma((4,)),
-            dma((2, 2)), dma((2, 2)), dma((2, 2)), dma((2, 2)),
-            dma((9, 4)), dma((9, 4)), dma((9, 4)), dma((9, 4)),
-            dma((4,)), dma((4,)), dma((2, 2)), dma((2, 2)), dma((2, 4)), dma((2, 4)),
-            dma((2, 4)), dma((2, 4)), dma((4,)), dma((4,)), dma((8,)),
+            dma(()), dma((2, 3)), dma(()), dma((4,)), dma(()), dma(()),
+            dma(()), dma((2, 2)), dma(()), dma((2,)),
+            dma((4,)), dma((4, 3)),
+            dma(()), dma(()), dma(()), dma((3,)), dma(()), dma((2,)),
+            dma(()), dma(()), dma(()), dma(()), dma((8,)),
             pltpu.VMEM(x.shape, BF16), pltpu.VMEM(gain.shape, F32), pltpu.VMEM(wq.shape, BF16),
             pltpu.VMEM(wk.shape, BF16), pltpu.VMEM(wv.shape, BF16), pltpu.VMEM(wo.shape, BF16),
         ],

time: 57.7 us -> 55 us (0.953); the launches traced: 56.6 us -> 54.8 us
  Pallas kernels: 56.6 us -> 54.8 us
    pallas_call x1, Pallas kernels: 54.7 us -> 52.9 us  [layer(): pl.pallas_call(layer_kernel, name='layer', out_shape=(jax.ShapeDtypeStruc...]
where the time goes in v6:
time: 55 us; the launch traced here: 54.8 us
  Pallas kernels  54.8 us (100%)
    pallas_call x1, Pallas kernels, layer(): pl.pallas_call(layer_kernel, name='layer', out_shape=(jax.ShapeDtypeStruc...  52.9 us
    pallas_call x1, Pallas kernels, mix(): pl.pallas_call(mix_kernel, name='mix', out_shape=jax.ShapeDtypeStruct((2...  1.92 us

profile of v6, /device:TPU:96, one launch (start us, length us, event | category | flops | bytes accessed | tf_op | source)
XLA Modules:
  0.0 54.8 jit_solution(18381252278634596876)
XLA Ops:
  0.0 52.9 %layer.1 = (bf16[16,96,128]{2,1,0:T(8,128)(2,1)S(1)}, bf16[4,4,64,2048]{3,2,1,0:T(8,128)(2,1)S(1)}) custom-call(bf16[192,2048]{1,0:T(8,128)(2,1)} %bitcast.10, f32[1,2048]{1,0:T(1,128)} %bitcast.13, bf16[64,256]{1,0:T(8,128)(2,1)} %bitcast.11, bf16[16,256]{1,0:T(8,128)(2,1)} %bitcast.14, bf16[16,256]{1,0:T(8,128)(2,1)} %bitcast.15, bf16[64,256]{1,0:T(8,128)(2,1)} %wo_hbm.1, ...), custom_call_target="tpu_custom_call" | custom-call | tf_op jit(solution)/shard_map/layer/pallas_call | solution.py:492
  52.9 1.9 %mix.1 = bf16[192,2048]{1,0:T(8,128)(2,1)} custom-call(bf16[16,96,128]{2,1,0:T(8,128)(2,1)S(1)} %get-tuple-element.7.ho_ref, bf16[1024,2048]{1,0:T(8,128)(2,1)S(1)} %bitcast.9), custom_call_target="tpu_custom_call" | custom-call | tf_op jit(solution)/shard_map/mix/pallas_call | solution.py:551

commit v7 on v6

--- a/solution.py
+++ b/solution.py
@@ -38,7 +38,7 @@
 def layer_kernel(
     x_hbm, gain_hbm, wq_hbm, wk_hbm, wv_hbm, wo_hbm, b_hbm, g_hbm,
     ho_ref, wo_ref,
-    qv_ref, kk_ref, keys_t, qa, vv, tri, part, rsum, acc, car, stage, h_s, h_r, b_ref, g_all,
+    qv_ref, kk_ref, keys_t, qa, vv, tri, part, rsum, stage, h_s, h_r, b_ref, g_all,
     packs, w_all, xg, stage_qv, stage_k,
     wa_s, wa_r, wb_s, wb_r, wc_s, wc_r, xd_s, xd_r, xf_s, xf_r, a_s, a_r,
     oz_s, oz_r, oy_s, oy_r, ox_s, ox_r, of_s, of_r, oc_s, oc_r, local_sem,
@@ -102,11 +102,12 @@
     def oz_out(dz):
         return rcopy(wo_in, oz(0, every), oz_s, oz_r, at(dz=dz))
 
-    third = rows // 3
-    parts = (
-        (pl.ds(0, 2 * third), pl.ds(2 * third, third)),
-        (pl.ds(third, 2 * third), pl.ds(0, third)),
+    sixth = rows // 6
+    spans = (
+        ((0, 3 * sixth), (3 * sixth, 2 * sixth), (5 * sixth, sixth)),
+        ((3 * sixth, 3 * sixth), (sixth, 2 * sixth), (0, sixth)),
     )
+    parts = tuple(tuple(pl.ds(*span) for span in side) for side in spans)
 
     def x_out(d, i):
         p = parts[d][i]
@@ -169,7 +170,7 @@
                 go(w_second(side, 0, o))
         for dz in (2, 1, 3):
             go(oz_out(dz))
-        for i in (0, 1):
+        for i in (0, 1, 2):
             for d in (0, 1):
                 go(x_out(d, i))
     with jax.named_scope("wait_wfirst"):
@@ -292,19 +293,14 @@
         rsum[i, j] = carry
 
     def finish(i):
-        acc[...] = part[i, i]
-        car[...] = rsum[i, i]
-
-        def add(n, _):
-            j = i - 1 - n
-            acc[...] += jnp.exp2(-car[...])[:, 0:HEAD_DIM] * part[i, j]
-            car[...] += rsum[i, j]
-            return 0
-
-        lax.fori_loop(0, i, add, 0)
+        a, later = part[i, i], rsum[i, i]
+        for n in range(1, RING):
+            j = jnp.maximum(i - n, 0)
+            there = jnp.where(i >= n, 1.0, 0.0).astype(F32)
+            a = a + (jnp.exp2(-later) * there)[:, 0:HEAD_DIM] * part[i, j]
+            later = later + rsum[i, j]
         pair_gain = g_all[0:1, block_rows(lax.div(me, 2), 128)]
         own_gain = jnp.where(lax.rem(me, 2) == 0, pair_gain[:, 0:64], pair_gain[:, 64:128])
-        a = acc[...]
         scaled = a * lax.rsqrt(jnp.mean(a * a, axis=-1, keepdims=True) + EPS)
         head = (scaled * own_gain).astype(BF16)
         for yy in range(RING):
@@ -361,25 +357,27 @@
             x_in(d, 0).wait_recv()
             for i in (0, 1):
                 go(far_z(d, i))
-    with jax.named_scope("chunk12"):
-        chunk(
-            jnp.concatenate([xg[0, parts[0][0]], xg[1, parts[1][0]]], axis=0),
-            ((3, 0, 2 * third), (1, third, 2 * third)),
-            rows,
-        )
+    def near_chunk(i, place):
+        with jax.named_scope("chunk_near%d" % i):
+            chunk(
+                jnp.concatenate([xg[0, parts[0][i]], xg[1, parts[1][i]]], axis=0),
+                ((3, *spans[0][i]), (1, *spans[1][i])),
+                place,
+            )
+
+    near_chunk(0, rows)
+    with jax.named_scope("wait_x1"):
+        x_in(0, 1).wait_recv()
+        x_in(1, 1).wait_recv()
+    near_chunk(1, rows + 6 * sixth)
     with jax.named_scope("prepare_own"):
         prepare(0)
     with jax.named_scope("diagonal_own"):
         diagonal(0)
-    with jax.named_scope("wait_x1"):
-        x_in(0, 1).wait_recv()
-        x_in(1, 1).wait_recv()
-    with jax.named_scope("chunk34"):
-        chunk(
-            jnp.concatenate([xg[0, parts[0][1]], xg[1, parts[1][1]]], axis=0),
-            ((3, 2 * third, third), (1, 0, third)),
-            rows + 4 * third,
-        )
+    with jax.named_scope("wait_x2"):
+        x_in(0, 2).wait_recv()
+        x_in(1, 2).wait_recv()
+    near_chunk(2, rows + 10 * sixth)
     with jax.named_scope("wait_oyfar"):
         settle(oy_r.at[2], RING * wo_rows)
         for d in (0, 1):
@@ -426,7 +424,7 @@
         go(oc(2))
     with jax.named_scope("finish_early"):
 
-        @pl.loop(0, far)
+        @pl.loop(0, jnp.where(far < RING - 1, far, 1))
         def _(i):
             finish(i)
 
@@ -436,20 +434,25 @@
         diagonal(2)
     with jax.named_scope("blocks_far"):
 
-        @pl.loop(0, RING)
+        @pl.loop(0, far)
         def _(i):
-            @pl.when(i < far)
-            def _():
-                pair(2, i - z + RING)
+            pair(2, i - z + RING)
+
+        finish(far)
+
+        @pl.loop(0, RING - 1)
+        def _(n):
+            dz = jnp.where(n == 0, 1, jnp.where(n == 1, 0, 3))
+            i = place(dz)
 
             @pl.when(i > far)
             def _():
-                pair(2, i - z + RING)
+                pair(2, dz)
                 finish(i)
 
-            @pl.when(i == far)
-            def _():
-                finish(i)
+        @pl.loop(1, jnp.where(far < RING - 1, 1, far))
+        def _(i):
+            finish(i)
 
     whole_w = wo_ref.at[:, :, :, pl.ds(0, RING * depth)]
     ho_rows = (RING * RING - 1) * half
@@ -507,8 +510,6 @@
             pltpu.VMEM((BLOCK_K, BLOCK_K), BF16),
             pltpu.VMEM((RING, RING, BLOCK_Q, HEAD_DIM), F32),
             pltpu.VMEM((RING, RING, BLOCK_Q, 128), F32),
-            pltpu.VMEM((BLOCK_Q, HEAD_DIM), F32),
-            pltpu.VMEM((BLOCK_Q, 128), F32),
             pltpu.VMEM((RING * RING, rows // 2, 2 * HEAD_DIM), BF16),
             dma(()), dma(()),
             pltpu.VMEM(bias.shape, F32), pltpu.VMEM(out_gain.shape, F32),
@@ -518,7 +519,7 @@
             pltpu.VMEM((RING, RING * rows, 128), BF16),
             pltpu.VMEM((RING * rows // 2, 128), BF16),
             dma(()), dma((2, 3)), dma(()), dma((4,)), dma(()), dma(()),
-            dma(()), dma((2, 2)), dma(()), dma((2,)),
+            dma(()), dma((2, 3)), dma(()), dma((2,)),
             dma((4,)), dma((4, 3)),
             dma(()), dma(()), dma(()), dma((3,)), dma(()), dma((2,)),
             dma(()), dma(()), dma(()), dma(()), dma((8,)),
@@ -531,7 +532,7 @@
     )(*operands)
 
 
-def mix_kernel(ho_ref, wo_ref, o_ref, lhs):
+def mix_kernel(ho_ref, wo_ref, o_hbm, lhs, o_ref, sems):
     heads, half, _ = ho_ref.shape
     for n in range(0, heads, 2):
         a, b = ho_ref[n], ho_ref[n + 1]
@@ -539,10 +540,18 @@
         lhs[0:half, cols] = jnp.concatenate([a[:, 0:64], b[:, 0:64]], axis=1)
         lhs[half : 2 * half, cols] = jnp.concatenate([a[:, 64:128], b[:, 64:128]], axis=1)
     width = o_ref.shape[1]
-    for n in range(0, width, 512):
-        o_ref[:, n : n + 512] = jnp.dot(
-            lhs[...], wo_ref[:, n : n + 512], preferred_element_type=F32
-        ).astype(BF16)
+    out = []
+    for n in range(width // MIX):
+        cols = slice(n * MIX, (n + 1) * MIX)
+        o_ref[:, cols] = jnp.dot(lhs[...], wo_ref[:, cols], preferred_element_type=F32).astype(BF16)
+        copy = pltpu.make_async_copy(o_ref.at[:, cols], o_hbm.at[:, cols], sems.at[n])
+        copy.start()
+        out.append(copy)
+    for copy in out:
+        copy.wait()
+
+
+MIX = 512
 
 
 def mix(ho, wo):
@@ -553,8 +562,12 @@
         name="mix",
         out_shape=jax.ShapeDtypeStruct((2 * half, wo.shape[1]), BF16),
         in_specs=[vmem] * 2,
-        out_specs=vmem,
-        scratch_shapes=[pltpu.VMEM((2 * half, heads * HEAD_DIM), BF16)],
+        out_specs=pl.BlockSpec(memory_space=pl.ANY),
+        scratch_shapes=[
+            pltpu.VMEM((2 * half, heads * HEAD_DIM), BF16),
+            pltpu.VMEM((2 * half, wo.shape[1]), BF16),
+            pltpu.SemaphoreType.DMA((wo.shape[1] // MIX,)),
+        ],
         compiler_params=pltpu.CompilerParams(vmem_limit_bytes=16 << 20),
     )(ho, wo)
 

time: 55 us -> 54.4 us (0.989)
  Pallas kernels: 54.8 us -> 53.8 us
    pallas_call x1, Pallas kernels: 52.9 us -> 52 us  [layer(): pl.pallas_call(layer_kernel, name='layer', out_shape=(jax.ShapeDtypeStruc...]
where the time goes in v7:
time: 54.4 us; the launch traced here: 54 us
  Pallas kernels  53.8 us (99%)
    pallas_call x1, Pallas kernels, layer(): pl.pallas_call(layer_kernel, name='layer', out_shape=(jax.ShapeDtypeStruc...  52 us
    pallas_call x1, Pallas kernels, mix(): pl.pallas_call(mix_kernel, name='mix', out_shape=jax.ShapeDtypeStruct((2...  1.76 us

profile of v7, /device:TPU:96, one launch (start us, length us, event | category | flops | bytes accessed | tf_op | source)
XLA Modules:
  0.0 54.0 jit_solution(10117802082114827021)
XLA Ops:
  0.0 52.0 %layer.1 = (bf16[16,96,128]{2,1,0:T(8,128)(2,1)S(1)}, bf16[4,4,64,2048]{3,2,1,0:T(8,128)(2,1)S(1)}) custom-call(bf16[192,2048]{1,0:T(8,128)(2,1)} %bitcast.10, f32[1,2048]{1,0:T(1,128)} %bitcast.13, bf16[64,256]{1,0:T(8,128)(2,1)} %bitcast.11, bf16[16,256]{1,0:T(8,128)(2,1)} %bitcast.14, bf16[16,256]{1,0:T(8,128)(2,1)} %bitcast.15, bf16[64,256]{1,0:T(8,128)(2,1)} %wo_hbm.1, ...), custom_call_target="tpu_custom_call" | custom-call | tf_op jit(solution)/shard_map/layer/pallas_call | solution.py:495
  52.0 1.8 %mix.1 = bf16[192,2048]{1,0:T(8,128)(2,1)} custom-call(bf16[16,96,128]{2,1,0:T(8,128)(2,1)S(1)} %get-tuple-element.7.ho_ref, bf16[1024,2048]{1,0:T(8,128)(2,1)S(1)} %bitcast.9), custom_call_target="tpu_custom_call" | custom-call | tf_op jit(solution)/shard_map/mix/pallas_call | solution.py:560

commit v8 on v7

--- a/solution.py
+++ b/solution.py
@@ -404,6 +404,9 @@
         prepare(3)
         prepare(1)
     far_chunk(0)
+    with jax.named_scope("diagonal_near"):
+        diagonal(3)
+        diagonal(1)
     far_chunk(1)
     with jax.named_scope("wait_ox2"):
         settle(ox_r.at[1], 2 * RING * wo_rows)
@@ -412,16 +415,11 @@
         go(oc(3))
         go(oc(1))
     with jax.named_scope("blocks_near"):
-        diagonal(3)
-        diagonal(1)
         pair(0, 3)
         pair(0, 1)
         pair(3, 1)
 
     far = place(2)
-    with jax.named_scope("wait_oxfar"):
-        settle(of_r, RING * RING * wo_rows)
-        go(oc(2))
     with jax.named_scope("finish_early"):
 
         @pl.loop(0, jnp.where(far < RING - 1, far, 1))
@@ -432,6 +430,9 @@
         prepare(2)
     with jax.named_scope("diagonal_far"):
         diagonal(2)
+    with jax.named_scope("wait_oxfar"):
+        settle(of_r, RING * RING * wo_rows)
+        go(oc(2))
     with jax.named_scope("blocks_far"):
 
         @pl.loop(0, far)

time: 54.4 us -> 54.3 us (level)
  no operation moved by 1% of the time
where the time goes in v8:
time: 54.3 us; the launch traced here: 53.7 us
  Pallas kernels  53.5 us (99%)
    pallas_call x1, Pallas kernels, layer(): pl.pallas_call(layer_kernel, name='layer', out_shape=(jax.ShapeDtypeStruc...  51.8 us
    pallas_call x1, Pallas kernels, mix(): pl.pallas_call(mix_kernel, name='mix', out_shape=jax.ShapeDtypeStruct((2...  1.76 us

profile of v8, /device:TPU:96, one launch (start us, length us, event | category | flops | bytes accessed | tf_op | source)
XLA Modules:
  0.0 53.7 jit_solution(6389112317729233536)
XLA Ops:
  0.0 51.8 %layer.1 = (bf16[16,96,128]{2,1,0:T(8,128)(2,1)S(1)}, bf16[4,4,64,2048]{3,2,1,0:T(8,128)(2,1)S(1)}) custom-call(bf16[192,2048]{1,0:T(8,128)(2,1)} %bitcast.10, f32[1,2048]{1,0:T(1,128)} %bitcast.13, bf16[64,256]{1,0:T(8,128)(2,1)} %bitcast.11, bf16[16,256]{1,0:T(8,128)(2,1)} %bitcast.14, bf16[16,256]{1,0:T(8,128)(2,1)} %bitcast.15, bf16[64,256]{1,0:T(8,128)(2,1)} %wo_hbm.1, ...), custom_call_target="tpu_custom_call" | custom-call | tf_op jit(solution)/shard_map/layer/pallas_call | solution.py:496
  51.8 1.8 %mix.1 = bf16[192,2048]{1,0:T(8,128)(2,1)} custom-call(bf16[16,96,128]{2,1,0:T(8,128)(2,1)S(1)} %get-tuple-element.7.ho_ref, bf16[1024,2048]{1,0:T(8,128)(2,1)S(1)} %bitcast.9), custom_call_target="tpu_custom_call" | custom-call | tf_op jit(solution)/shard_map/mix/pallas_call | solution.py:561
